TPU v7x, 512 devices: a whole 4x4x16 slice. The times are simulated.
512 devices in a mesh: sp: 16 (over z), fs: 4 (over y), tp: 8 (over x, core).
Axes of the slice: x: 4, y: 4, z: 16, core: 2. Of those that a mesh axis runs over, the one named last changes fastest.
Arguments:
- tokens: bfloat16 [4, 8192, 2048], P('fs', 'sp'), may hold values from -6 to 6
- input_gain: float32 [2048], replicated, may hold values from 0.1 to 1.9
- weight_gate: bfloat16 [2048, 2048], P('sp', 'tp'), may hold values from -0.125 to 0.125
- weight_input: bfloat16 [2048, 2048], P('sp', 'tp'), may hold values from -0.125 to 0.125
- weight_write: bfloat16 [2048, 1024], P('sp', 'tp'), may hold values from -0.125 to 0.125
- weight_read: bfloat16 [2048, 1024], P('sp', 'tp'), may hold values from -0.125 to 0.125
- weight_step: bfloat16 [2048, 32], P('sp', 'tp'), may hold values from -0.125 to 0.125
- weight_value: bfloat16 [2048, 2048], P('sp', 'tp'), may hold values from -0.125 to 0.125
- weight_sigmoid: bfloat16 [2048, 2048], P('sp', 'tp'), may hold values from -0.125 to 0.125
- filter_input: bfloat16 [4, 2048], P(None, 'tp'), may hold values from -3 to 3
- filter_write: bfloat16 [4, 1024], P(None, 'tp'), may hold values from -3 to 3
- filter_read: bfloat16 [4, 1024], P(None, 'tp'), may hold values from -3 to 3
- step_bias: float32 [32], P('tp'), may hold values from -4.5 to -3.5
- rate_log: float32 [32], P('tp'), as said below
- skip_gain: float32 [32], P('tp'), may hold values from 0.1 to 1.9
- output_gain: float32 [2048], P('tp'), may hold values from 0.1 to 1.9
- opening_state: float32 [4, 32, 64, 128], P('fs', 'tp'), may hold values from -12 to 12
- decay_shift: float32 [4, 32, 8192], P('fs', 'tp', 'sp'), may hold values from -3 to 0, as said below
- depth_filter: bfloat16 [31, 2048], P(None, 'tp'), may hold values from -40 to 40
- channel_gain: float32 [2048], P('tp'), may hold values from 0.1 to 1.9
- unproject_state: bfloat16 [2048, 2048], P('tp', 'sp'), may hold values from -0.09375 to 0.09375
- unproject_filter: bfloat16 [2048, 2048], P('tp', 'sp'), may hold values from -0.09375 to 0.09375
Outputs:
- mixed: bfloat16 [4, 8192, 2048], P('fs', ('sp', 'tp'))
Inputs may be any that keep to these rules, and one draw needn't show every extreme that they name: `rate_log`: logarithms of the heads' decay rates. `decay_shift`: Non-positive.
All inputs are finite; a program needn't handle non-finite values.
Results may differ from a plain program's by a relative error of at most 0.018.
Values may be sent and summed in bfloat16 or wider, within the bound.
A program may use at most 64 MiB of HBM per device.

v0:
```python
from functools import partial

import jax
import jax.numpy as jnp
from jax import lax
from jax.sharding import PartitionSpec as P

HEAD_DIM = 64
STATE = 128
CM = 2048
BLOCK = 128


def in_one_piece(arrays, axis, dim, along):
    widths = [a.shape[along] for a in arrays]
    both = jnp.concatenate(arrays, axis=along)
    result = lax.all_gather(both, axis, axis=dim, tiled=True)
    return tuple(jnp.split(result, [sum(widths[:k]) for k in range(1, len(widths))], axis=along))


def passed_along(array, axis, by):
    length = lax.axis_size(axis)
    pairs = [(i, i + by) for i in range(length) if 0 <= i + by < length]
    return lax.ppermute(array, axis, pairs)


def laid_out(parts, dim):
    dims = list(parts.shape[1:])
    dims[dim] *= parts.shape[0]
    return jnp.moveaxis(parts, 0, dim).reshape(dims)


def from_everyone(array, axis):
    copies = jnp.broadcast_to(array, (lax.axis_size(axis), *array.shape))
    return lax.all_to_all(copies, axis, split_axis=0, concat_axis=0, tiled=True)


def collect(array, axis, dim):
    return laid_out(from_everyone(array, axis), dim)


def over_copies(array, axis):
    return from_everyone(array, axis).sum(axis=0)


def together(arrays, axis):
    ends = [0]
    for a in arrays:
        ends.append(ends[-1] + a.size)
    subtotal = over_copies(jnp.concatenate([a.ravel() for a in arrays]), axis)
    return tuple((subtotal[b:e].reshape(a.shape) for a, b, e in zip(arrays, ends, ends[1:])))


def split_up(array, dim, length):
    before, after = (array.shape[:dim], array.shape[dim + 1 :])
    return jnp.moveaxis(array.reshape(*before, length, -1, *after), dim, 0)


def summed_on_arrival(array, axis, dim):
    length = lax.axis_size(axis)
    parts = lax.all_to_all(split_up(array, dim, length), axis, 0, 0, tiled=True)
    return jnp.sum(parts.astype(jnp.float32), axis=0)


def causal_filter(border, values, kernel):
    extended = jnp.concatenate([border, values], axis=0).astype(jnp.float32)
    weights = kernel.astype(jnp.float32)
    row_count = values.shape[0]
    result = jnp.zeros(values.shape, jnp.float32)
    for offset in range(kernel.shape[0]):
        result = result + weights[offset] * extended[offset : offset + row_count]
    return result


def block_step(direct_gain, memory, pieces):
    input_block, write_block, read_block, step_block, log_block = pieces
    head_count = input_block.shape[1]
    per_group = head_count // write_block.shape[1]
    running = jnp.cumsum(log_block, axis=0)
    write_heads = jnp.repeat(write_block, per_group, axis=1)
    read_heads = jnp.repeat(read_block, per_group, axis=1)
    scores = jnp.einsum("lhn,shn->hls", read_heads, write_heads)
    spread = running.T[:, :, None] - running.T[:, None, :]
    row_index = lax.broadcasted_iota(jnp.int32, spread.shape, 1)
    col_index = lax.broadcasted_iota(jnp.int32, spread.shape, 2)
    decays = jnp.exp(jnp.where(row_index >= col_index, spread, -jnp.inf))
    scaled_inputs = input_block * step_block[:, :, None]
    inside = jnp.einsum("hls,shp->lhp", scores * decays, scaled_inputs)
    carried = jnp.exp(running)[:, :, None] * jnp.einsum("lhn,hpn->lhp", read_heads, memory)
    output = inside + carried + direct_gain[None, :, None] * input_block
    to_end = jnp.exp(running[-1][None, :] - running)
    fresh_terms = jnp.einsum("lhp,lhn->hpn", scaled_inputs * to_end[:, :, None], write_heads)
    new_memory = jnp.exp(running[-1])[:, None, None] * memory + fresh_terms
    return (new_memory, output)


def per_device(
    tokens,
    input_gain,
    weight_gate,
    weight_input,
    weight_write,
    weight_read,
    weight_step,
    weight_value,
    weight_sigmoid,
    filter_input,
    filter_write,
    filter_read,
    step_bias,
    rate_log,
    skip_gain,
    output_gain,
    opening_state,
    decay_shift,
    depth_filter,
    channel_gain,
    unproject_state,
    unproject_filter,
):
    row_count = tokens.shape[1]
    source = tokens[0].astype(jnp.float32)
    normed = (
        source * lax.rsqrt(jnp.mean(source * source, axis=-1, keepdims=True) + 1e-06) * input_gain
    ).astype(jnp.bfloat16)
    pieces = in_one_piece(
        (
            weight_gate,
            weight_input,
            weight_write,
            weight_read,
            weight_step,
            weight_value,
            weight_sigmoid,
        ),
        "sp",
        0,
        1,
    )
    sums = tuple((jnp.dot(normed, piece, preferred_element_type=jnp.float32) for piece in pieces))
    gate_values, input_values, write_values, read_values, step_values, value_rows, sigmoid_rows = (
        total.astype(jnp.bfloat16) for total in sums
    )
    glu_rows = (
        value_rows.astype(jnp.float32) * jax.nn.sigmoid(sigmoid_rows.astype(jnp.float32))
    ).astype(jnp.bfloat16)
    short_rim = filter_input.shape[0] - 1
    long_rim = depth_filter.shape[0] - 1
    borders = passed_along(
        (
            input_values[row_count - short_rim :],
            write_values[row_count - short_rim :],
            read_values[row_count - short_rim :],
            glu_rows[row_count - long_rim :],
        ),
        "sp",
        1,
    )
    mixed_input = jax.nn.silu(causal_filter(borders[0], input_values, filter_input)).astype(
        jnp.bfloat16
    )
    mixed_write = jax.nn.silu(causal_filter(borders[1], write_values, filter_write)).astype(
        jnp.bfloat16
    )
    mixed_read = jax.nn.silu(causal_filter(borders[2], read_values, filter_read)).astype(
        jnp.bfloat16
    )
    head_count = rate_log.shape[0]
    group_count = mixed_write.shape[1] // STATE
    step_sizes = jax.nn.softplus(step_values.astype(jnp.float32) + step_bias)
    log_rates = -step_sizes * jnp.exp(rate_log) + decay_shift[0].T
    inputs_float = mixed_input.astype(jnp.float32).reshape(row_count, head_count, HEAD_DIM)
    write_float = mixed_write.astype(jnp.float32).reshape(row_count, group_count, STATE)
    read_float = mixed_read.astype(jnp.float32).reshape(row_count, group_count, STATE)
    block_count = row_count // BLOCK
    blocked = tuple(
        (
            array.reshape((block_count, BLOCK) + array.shape[1:])
            for array in (inputs_float, write_float, read_float, step_sizes, log_rates)
        )
    )
    zero_memory = jnp.zeros((head_count, HEAD_DIM, STATE), jnp.float32)
    local_memory, outputs = lax.scan(partial(block_step, skip_gain), zero_memory, blocked)
    outputs = outputs.reshape(row_count, head_count, HEAD_DIM)
    running = jnp.cumsum(log_rates, axis=0)
    total_decay = running[-1]
    totals = collect(total_decay[None, :], "sp", 0)
    inclusive = jnp.cumsum(totals, axis=0)
    exclusive = inclusive - totals
    my_index = lax.axis_index("sp")
    before = lax.dynamic_slice_in_dim(exclusive, my_index, 1, 0)[0]
    piece = collect(local_memory[None].astype(jnp.bfloat16), "sp", 0).astype(jnp.float32)
    piece_rows = piece.shape[0]
    owners = jnp.arange(piece_rows, dtype=jnp.int32)
    weights = jnp.exp(
        jnp.where((owners < my_index)[:, None], before[None, :] - inclusive, -jnp.inf)
    )
    leading_memory = jnp.zeros_like(local_memory) + jnp.einsum("jh,jhpn->hpn", weights, piece)
    entering = opening_state[0] * jnp.exp(before)[:, None, None] + leading_memory
    read_heads = jnp.repeat(read_float, head_count // group_count, axis=1)
    outputs = outputs + jnp.exp(running)[:, :, None] * jnp.einsum(
        "lhn,hpn->lhp", read_heads, entering
    )
    gated = outputs.reshape(row_count, -1) * jax.nn.silu(gate_values.astype(jnp.float32))
    grouped = gated.reshape(row_count, group_count, -1)
    grouped = grouped * lax.rsqrt(jnp.mean(grouped * grouped, axis=-1, keepdims=True) + 1e-06)
    state_out = (grouped.reshape(row_count, -1) * output_gain).astype(jnp.bfloat16)
    filtered = causal_filter(borders[3], glu_rows, depth_filter)
    channel_sums = together((jnp.sum(filtered, axis=1), jnp.sum(filtered * filtered, axis=1)), "tp")
    mean_value = channel_sums[0] / CM
    mean_square = channel_sums[1] / CM
    variance = mean_square - mean_value * mean_value
    normal_rows = (
        (filtered - mean_value[:, None]) * lax.rsqrt(variance + 1e-05)[:, None] * channel_gain
    )
    filter_out = jax.nn.silu(normal_rows).astype(jnp.bfloat16)
    full_state, full_filter = in_one_piece((unproject_state, unproject_filter), "sp", 1, 0)
    summed = summed_on_arrival(
        (
            jnp.dot(state_out, full_state, preferred_element_type=jnp.float32)
            + jnp.dot(filter_out, full_filter, preferred_element_type=jnp.float32)
        ).astype(jnp.bfloat16),
        "tp",
        0,
    )
    return summed.astype(jnp.bfloat16)[None]


def solution(mesh):
    in_specs = (
        P("fs", "sp", None),
        P(),
        P("sp", "tp"),
        P("sp", "tp"),
        P("sp", "tp"),
        P("sp", "tp"),
        P("sp", "tp"),
        P("sp", "tp"),
        P("sp", "tp"),
        P(None, "tp"),
        P(None, "tp"),
        P(None, "tp"),
        P("tp"),
        P("tp"),
        P("tp"),
        P("tp"),
        P("fs", "tp", None, None),
        P("fs", "tp", "sp"),
        P(None, "tp"),
        P("tp"),
        P("tp", "sp"),
        P("tp", "sp"),
    )
    out_specs = P("fs", ("sp", "tp"), None)
    return jax.shard_map(
        per_device, mesh=mesh, in_specs=in_specs, out_specs=out_specs, check_vma=False
    )
```

profile of v0, /device:TPU:1, one launch (start us, length us, event | category | flops | bytes accessed | tf_op | source)
XLA Modules:
  0.0 328.9 jit_solution(4849453516563715798)
XLA Ops:
  7.5 1.9 concatenate.21
  11.5 2.1 fusion.31
  15.0 1.8 fusion.33
  16.8 76.3 %all-gather.3.cloned.1.call-done = bf16[2048,1284]{1,0:T(8,128)(2,1)} async-done(((bf16[128,1284]{1,0:T(8,128)(2,1)}), bf16[2048,1284]{1,0:T(8,128)(2,1)}) %all-gather.3.cloned.1.call-update) | async-done | bytes 5259280 | tf_op jit(solution)/shard_map/all_gather | solution.py:17
  93.1 3.0 fusion.44
  97.8 2.3 collective-permute-start.3
  100.8 3.4 %collective-permute-start.2 = (bf16[3,128]{1,0:T(4,128)(2,1)S(1)}, bf16[3,128]{1,0:T(4,128)(2,1)S(1)}, u32[]{:S(2)}, u32[]{:S(2)}) collective-permute-start(bf16[3,128]{1,0:T(4,128)(2,1)S(1)} %slice.403), channel_id=1, source_target_pairs={{0,32},{32,64},{64,96},{96,128},{128,160},{160,192},{192,224},{224... | collective-permute-start | bytes 2312 | tf_op jit(solution)/shard_map/ppermute | solution.py:24
  105.0 3.3 %collective-permute-start = (bf16[3,256]{1,0:T(4,128)(2,1)S(1)}, bf16[3,256]{1,0:T(4,128)(2,1)S(1)}, u32[]{:S(2)}, u32[]{:S(2)}) collective-permute-start(bf16[3,256]{1,0:T(4,128)(2,1)S(1)} %slice.390), channel_id=1, source_target_pairs={{0,32},{32,64},{64,96},{96,128},{128,160},{160,192},{192,224},{224... | collective-permute-start | bytes 4616 | tf_op jit(solution)/shard_map/ppermute | solution.py:24
  109.1 3.5 %collective-permute-start.1 = (bf16[3,128]{1,0:T(4,128)(2,1)S(1)}, bf16[3,128]{1,0:T(4,128)(2,1)S(1)}, u32[]{:S(2)}, u32[]{:S(2)}) collective-permute-start(bf16[3,128]{1,0:T(4,128)(2,1)S(1)} %slice.398), channel_id=1, source_target_pairs={{0,32},{32,64},{64,96},{96,128},{128,160},{160,192},{192,224},{224... | collective-permute-start | bytes 2312 | tf_op jit(solution)/shard_map/ppermute | solution.py:24
  113.3 1.2 reduce-window.6
  116.6 6.9 %all-to-all-start = ((f32[16,1,4]{2,1,0:T(1,128)}), f32[16,1,4]{2,1,0:T(1,128)S(1)}, u32[]{:S(2)}, u32[]{:S(2)}) async-start(f32[16,1,4]{2,1,0:T(1,128)} %broadcast_in_dim.43), calls=%async_computation | async-start | bytes 16384 | tf_op jit(solution)/shard_map/all_to_all | solution.py:35
  124.7 1.1 fusion.107
  125.9 1.5 reshape.145
  127.4 1.1 copy.141
  129.7 3.7 %fusion.123 = (f32[512]{0:T(512)S(1)}, f32[512]{0:T(512)S(1)}, f32[512,256]{1,0:T(8,128)}) fusion(f32[542,256]{1,0:T(8,128)S(1)} %maximum_convert_fusion, f32[256]{0:T(256)S(1)} %bitcast.219, f32[256]{0:T(256)S(1)} %bitcast.218, f32[256]{0:T(256)S(1)} %bitcast.217, f32[256]{0:T(256)S(1)} %bitcast.216, f32[256]{0:T(256)S(1)} %bitcast.215, ...), kind=kLoop, calls=%fused_computation.223 | loop fusion | flops 8387584 | bytes 16813056 | tf_op jit(solution)/shard_map/reduce_sum | solution.py:209
  133.4 1.4 all-to-all-done
  135.5 10.7 %all-to-all-start.2 = ((f32[8,1,1024]{2,1,0:T(1,128)}), f32[8,1,1024]{2,1,0:T(1,128)S(1)}, u32[]{:S(2)}, u32[]{:S(2)}) async-start(f32[8,1,1024]{2,1,0:T(1,128)} %broadcast_in_dim.47), calls=%async_computation.2 | async-start | bytes 65536 | tf_op jit(solution)/shard_map/all_to_all | solution.py:35
  146.2 28.8 %while.13 = (s32[]{:T(128)}, f32[4,64,128]{2,1,0:T(8,128)S(1)}, f32[4,128,4,64]{1,0,3,2:T(4,128)}, f32[4,128,4]{2,1,0:T(8,128)}, f32[4,128,4,64]{1,3,2,0:T(8,128...) while((s32[]{:T(128)}, f32[4,64,128]{2,1,0:T(8,128)S(1)}, ...), condition=%wide.region_3.4_spmd.clone, body=%wide.region_1.3_spmd.clone.sunk | while | flops 42696704 | bytes 1749224 | solution.py:183
  148.7 4.4 %dynamic_update_slice.6 = f32[4,128,4,64]{1,0,3,2:T(4,128)} dynamic-update-slice(f32[4,128,4,64]{1,0,3,2:T(4,128)} %get-tuple-element.303, f32[1,128,4,64]{1,0,3,2:T(1,128)S(1)} %bitcast.195, s32[]{:T(128)} %get-tuple-element.301, s32[]{:T(128)} %constant.58.clone.1..sunk, s32[]{:T(128)} %constant.58.clone.1..sunk, s32[]{:T(128)} %constant.58.clone.1..sunk) | dynamic-update-slice | bytes 262148 | tf_op jit(solution)/shard_map/while/body/jit(dynamic_update_index_in_dim)/dynamic_update_slice | solution.py:183
  155.9 4.4 %dynamic_update_slice.6 = f32[4,128,4,64]{1,0,3,2:T(4,128)} dynamic-update-slice(f32[4,128,4,64]{1,0,3,2:T(4,128)} %get-tuple-element.303, f32[1,128,4,64]{1,0,3,2:T(1,128)S(1)} %bitcast.195, s32[]{:T(128)} %get-tuple-element.301, s32[]{:T(128)} %constant.58.clone.1..sunk, s32[]{:T(128)} %constant.58.clone.1..sunk, s32[]{:T(128)} %constant.58.clone.1..sunk) | dynamic-update-slice | bytes 262148 | tf_op jit(solution)/shard_map/while/body/jit(dynamic_update_index_in_dim)/dynamic_update_slice | solution.py:183
  163.2 4.4 %dynamic_update_slice.6 = f32[4,128,4,64]{1,0,3,2:T(4,128)} dynamic-update-slice(f32[4,128,4,64]{1,0,3,2:T(4,128)} %get-tuple-element.303, f32[1,128,4,64]{1,0,3,2:T(1,128)S(1)} %bitcast.195, s32[]{:T(128)} %get-tuple-element.301, s32[]{:T(128)} %constant.58.clone.1..sunk, s32[]{:T(128)} %constant.58.clone.1..sunk, s32[]{:T(128)} %constant.58.clone.1..sunk) | dynamic-update-slice | bytes 262148 | tf_op jit(solution)/shard_map/while/body/jit(dynamic_update_index_in_dim)/dynamic_update_slice | solution.py:183
  170.4 4.4 %dynamic_update_slice.6 = f32[4,128,4,64]{1,0,3,2:T(4,128)} dynamic-update-slice(f32[4,128,4,64]{1,0,3,2:T(4,128)} %get-tuple-element.303, f32[1,128,4,64]{1,0,3,2:T(1,128)S(1)} %bitcast.195, s32[]{:T(128)} %get-tuple-element.301, s32[]{:T(128)} %constant.58.clone.1..sunk, s32[]{:T(128)} %constant.58.clone.1..sunk, s32[]{:T(128)} %constant.58.clone.1..sunk) | dynamic-update-slice | bytes 262148 | tf_op jit(solution)/shard_map/while/body/jit(dynamic_update_index_in_dim)/dynamic_update_slice | solution.py:183
  175.0 1.3 broadcast_in_dim.46
  176.3 9.3 %all-to-all-start.1 = ((bf16[16,1,4,64,128]{4,3,2,1,0:T(8,128)(2,1)}), bf16[16,1,4,64,128]{4,3,2,1,0:T(8,128)(2,1)S(1)}, u32[]{:S(2)}, u32[]{:S(2)}) async-start(bf16[16,1,4,64,128]{4,3,2,1,0:T(8,128)(2,1)} %broadcast_in_dim.46), calls=%async_computation.1 | async-start | bytes 2097152 | tf_op jit(solution)/shard_map/all_to_all | solution.py:35
  185.9 1.5 pad_maximum_fusion
  187.9 2.1 reshape.130
  190.0 46.7 %all-to-all-done.1 = bf16[16,1,4,64,128]{4,3,2,1,0:T(8,128)(2,1)S(1)} async-done(((bf16[16,1,4,64,128]{4,3,2,1,0:T(8,128)(2,1)}), bf16[16,1,4,64,128]{4,3,2,1,0:T(8,128)(2,1)S(1)}, u32[]{:S(2)}, u32[]{:S(2)}) %all-to-all-start.1) | async-done | bytes 1048608 | tf_op jit(solution)/shard_map/all_to_all | solution.py:35
  237.4 1.4 fusion.35
  239.0 2.1 multiply_reduce_fusion.1
  241.1 37.4 %all-gather.5.cloned.1.call-done = bf16[512,2048]{1,0:T(8,128)(2,1)} async-done(((bf16[512,128]{1,0:T(8,128)(2,1)}), bf16[512,2048]{1,0:T(8,128)(2,1)}) %all-gather.5.cloned.1.call-update) | async-done | bytes 2097168 | tf_op jit(solution)/shard_map/all_gather | solution.py:17
  278.5 2.1 fusion.50
  281.5 39.5 %all_to_all.21 = bf16[8,64,2048]{2,1,0:T(8,128)(2,1)S(1)} all-to-all(bf16[8,64,2048]{2,1,0:T(8,128)(2,1)S(1)} %bitcast.193), channel_id=1, replica_groups=mesh['sp'=16,'fs'=4,'tp'=8] {'tp'}, dimensions={0} | all-to-all | bytes 4194304 | tf_op jit(solution)/shard_map/all_to_all | solution.py:61
  (167 shorter events, 28.5 us)
Async XLA Ops:
  6.5 8.4 %copy-start = (bf16[1,512,2048]{2,1,0:T(8,128)(2,1)S(1)}, bf16[1,512,2048]{2,1,0:T(8,128)(2,1)}, u32[]{:S(2)}) copy-start(bf16[1,512,2048]{2,1,0:T(8,128)(2,1)} %param.24) | copy-start | bytes 6291460
  6.5 7.1 %copy-start.11 = (bf16[4,256]{1,0:T(4,128)(2,1)S(1)}, bf16[4,256]{1,0:T(4,128)(2,1)}, u32[]{:S(2)}) copy-start(bf16[4,256]{1,0:T(4,128)(2,1)} %param.33) | copy-start | bytes 6148
  6.5 7.1 %copy-start.7 = (bf16[31,256]{1,0:T(8,128)(2,1)S(1)}, bf16[31,256]{1,0:T(8,128)(2,1)}, u32[]{:S(2)}) copy-start(bf16[31,256]{1,0:T(8,128)(2,1)} %param.42) | copy-start | bytes 47620
  6.5 8.4 %copy-start.10 = (f32[2048]{0:T(1024)S(1)}, f32[2048]{0:T(1024)}, u32[]{:S(2)}) copy-start(f32[2048]{0:T(1024)} %param.25) | copy-start | bytes 24580
  6.5 86.6 %all-gather.3.cloned.1.call-start = ((), (), s32[]{:S(2)}) async-start(), calls=%async_computation.4 | async-start | bytes 6127616 | tf_op jit(solution)/shard_map/all_gather | solution.py:17
  16.8 79.3 %copy-start.1 = (bf16[512,2048]{1,0:T(8,128)(2,1)S(1)}, bf16[512,2048]{1,0:T(8,128)(2,1)}, u32[]{:S(2)}) copy-start(bf16[512,2048]{1,0:T(8,128)(2,1)} %fusion.33) | copy-start | bytes 6291460
  93.1 3.8 %copy-start.8 = (bf16[2048,1284]{1,0:T(8,128)(2,1)S(1)}, bf16[2048,1284]{1,0:T(8,128)(2,1)}, u32[]{:S(2)}) copy-start(bf16[2048,1284]{1,0:T(8,128)(2,1)} %all-gather.3.cloned.1.call-done) | copy-start | bytes 15777796
  97.7 7.2 %copy-start.5 = (bf16[512,256]{1,0:T(8,128)(2,1)}, bf16[512,256]{1,0:T(8,128)(2,1)S(1)}, u32[]{:S(2)}) copy-start(bf16[512,256]{1,0:T(8,128)(2,1)S(1)} %fusion.39) | copy-start | bytes 786436
  97.8 30.8 %collective-permute-start.3 = (bf16[30,256]{1,0:T(8,128)(2,1)S(1)}, bf16[30,256]{1,0:T(8,128)(2,1)S(1)}, u32[]{:S(2)}, u32[]{:S(2)}) collective-permute-start(bf16[30,256]{1,0:T(8,128)(2,1)S(1)} %slice.411), channel_id=1, source_target_pairs={{0,32},{32,64},{64,96},{96,128},{128,160},{160,192},{192,224},{224... | collective-permute-start | bytes 46088 | tf_op jit(solution)/shard_map/ppermute | solution.py:24
  100.8 22.7 %collective-permute-start.2 = (bf16[3,128]{1,0:T(4,128)(2,1)S(1)}, bf16[3,128]{1,0:T(4,128)(2,1)S(1)}, u32[]{:S(2)}, u32[]{:S(2)}) collective-permute-start(bf16[3,128]{1,0:T(4,128)(2,1)S(1)} %slice.403), channel_id=1, source_target_pairs={{0,32},{32,64},{64,96},{96,128},{128,160},{160,192},{192,224},{224... | collective-permute-start | bytes 2312 | tf_op jit(solution)/shard_map/ppermute | solution.py:24
  105.0 7.5 %copy-start.9 = (f32[1,4,512]{2,1,0:T(4,128)S(1)}, f32[1,4,512]{2,1,0:T(4,128)}, u32[]{:S(2)}) copy-start(f32[1,4,512]{2,1,0:T(4,128)} %param.41) | copy-start | bytes 24580
  105.0 7.5 %copy-start.24 = (f32[4]{0:T(128)S(1)}, f32[4]{0:T(128)}, u32[]{:S(2)}) copy-start(f32[4]{0:T(128)} %param.36) | copy-start | bytes 52
  105.0 19.7 %collective-permute-start = (bf16[3,256]{1,0:T(4,128)(2,1)S(1)}, bf16[3,256]{1,0:T(4,128)(2,1)S(1)}, u32[]{:S(2)}, u32[]{:S(2)}) collective-permute-start(bf16[3,256]{1,0:T(4,128)(2,1)S(1)} %slice.390), channel_id=1, source_target_pairs={{0,32},{32,64},{64,96},{96,128},{128,160},{160,192},{192,224},{224... | collective-permute-start | bytes 4616 | tf_op jit(solution)/shard_map/ppermute | solution.py:24
  109.1 14.7 %collective-permute-start.1 = (bf16[3,128]{1,0:T(4,128)(2,1)S(1)}, bf16[3,128]{1,0:T(4,128)(2,1)S(1)}, u32[]{:S(2)}, u32[]{:S(2)}) collective-permute-start(bf16[3,128]{1,0:T(4,128)(2,1)S(1)} %slice.398), channel_id=1, source_target_pairs={{0,32},{32,64},{64,96},{96,128},{128,160},{160,192},{192,224},{224... | collective-permute-start | bytes 2312 | tf_op jit(solution)/shard_map/ppermute | solution.py:24
  116.6 18.2 %all-to-all-start = ((f32[16,1,4]{2,1,0:T(1,128)}), f32[16,1,4]{2,1,0:T(1,128)S(1)}, u32[]{:S(2)}, u32[]{:S(2)}) async-start(f32[16,1,4]{2,1,0:T(1,128)} %broadcast_in_dim.43), calls=%async_computation | async-start | bytes 16384 | tf_op jit(solution)/shard_map/all_to_all | solution.py:35
  125.9 3.7 %copy-start.12 = (f32[1,256]{1,0:T(1,128)S(1)}, f32[1,256]{1,0:T(1,128)}, u32[]{:S(2)}) copy-start(f32[1,256]{1,0:T(1,128)} %get-tuple-element.204) | copy-start | bytes 3076
  125.9 3.7 %copy-start.13 = (f32[1,256]{1,0:T(1,128)S(1)}, f32[1,256]{1,0:T(1,128)}, u32[]{:S(2)}) copy-start(f32[1,256]{1,0:T(1,128)} %get-tuple-element.205) | copy-start | bytes 3076
  125.9 3.7 %copy-start.14 = (f32[1,256]{1,0:T(1,128)S(1)}, f32[1,256]{1,0:T(1,128)}, u32[]{:S(2)}) copy-start(f32[1,256]{1,0:T(1,128)} %get-tuple-element.175) | copy-start | bytes 3076
  125.9 3.7 %copy-start.15 = (f32[1,256]{1,0:T(1,128)S(1)}, f32[1,256]{1,0:T(1,128)}, u32[]{:S(2)}) copy-start(f32[1,256]{1,0:T(1,128)} %get-tuple-element.176) | copy-start | bytes 3076
  125.9 3.7 %copy-start.16 = (f32[1,256]{1,0:T(1,128)S(1)}, f32[1,256]{1,0:T(1,128)}, u32[]{:S(2)}) copy-start(f32[1,256]{1,0:T(1,128)} %get-tuple-element.177) | copy-start | bytes 3076
  125.9 3.7 %copy-start.17 = (f32[1,256]{1,0:T(1,128)S(1)}, f32[1,256]{1,0:T(1,128)}, u32[]{:S(2)}) copy-start(f32[1,256]{1,0:T(1,128)} %get-tuple-element.178) | copy-start | bytes 3076
  125.9 3.7 %copy-start.18 = (f32[1,256]{1,0:T(1,128)S(1)}, f32[1,256]{1,0:T(1,128)}, u32[]{:S(2)}) copy-start(f32[1,256]{1,0:T(1,128)} %get-tuple-element.179) | copy-start | bytes 3076
  125.9 3.7 %copy-start.19 = (f32[1,256]{1,0:T(1,128)S(1)}, f32[1,256]{1,0:T(1,128)}, u32[]{:S(2)}) copy-start(f32[1,256]{1,0:T(1,128)} %get-tuple-element.180) | copy-start | bytes 3076
  125.9 3.7 %copy-start.20 = (f32[1,256]{1,0:T(1,128)S(1)}, f32[1,256]{1,0:T(1,128)}, u32[]{:S(2)}) copy-start(f32[1,256]{1,0:T(1,128)} %get-tuple-element.181) | copy-start | bytes 3076
  125.9 3.7 %copy-start.21 = (f32[1,256]{1,0:T(1,128)S(1)}, f32[1,256]{1,0:T(1,128)}, u32[]{:S(2)}) copy-start(f32[1,256]{1,0:T(1,128)} %get-tuple-element.182) | copy-start | bytes 3076
  129.7 16.5 %copy-start.2 = (f32[4,128,4,64]{1,3,2,0:T(8,128)S(1)}, f32[4,128,4,64]{1,3,2,0:T(8,128)}, u32[]{:S(2)}) copy-start(f32[4,128,4,64]{1,3,2,0:T(8,128)} %copy.141) | copy-start | bytes 1572868
  129.7 16.5 %copy-start.25 = (f32[4]{0:T(128)S(1)}, f32[4]{0:T(128)}, u32[]{:S(2)}) copy-start(f32[4]{0:T(128)} %param.38) | copy-start | bytes 52
  135.5 39.5 %all-to-all-start.2 = ((f32[8,1,1024]{2,1,0:T(1,128)}), f32[8,1,1024]{2,1,0:T(1,128)S(1)}, u32[]{:S(2)}, u32[]{:S(2)}) async-start(f32[8,1,1024]{2,1,0:T(1,128)} %broadcast_in_dim.47), calls=%async_computation.2 | async-start | bytes 65536 | tf_op jit(solution)/shard_map/all_to_all | solution.py:35
  176.3 61.1 %copy-start.6 = (f32[1,4,64,128]{3,2,1,0:T(8,128)S(1)}, f32[1,4,64,128]{3,2,1,0:T(8,128)}, u32[]{:S(2)}) copy-start(f32[1,4,64,128]{3,2,1,0:T(8,128)} %param.40) | copy-start | bytes 393220
  176.3 60.4 %all-to-all-start.1 = ((bf16[16,1,4,64,128]{4,3,2,1,0:T(8,128)(2,1)}), bf16[16,1,4,64,128]{4,3,2,1,0:T(8,128)(2,1)S(1)}, u32[]{:S(2)}, u32[]{:S(2)}) async-start(bf16[16,1,4,64,128]{4,3,2,1,0:T(8,128)(2,1)} %broadcast_in_dim.46), calls=%async_computation.1 | async-start | bytes 2097152 | tf_op jit(solution)/shard_map/all_to_all | solution.py:35
  185.7 92.8 %all-gather.5.cloned.1.call-start = ((), (), s32[]{:S(2)}) async-start(), calls=%async_computation.5 | async-start | bytes 2228224 | tf_op jit(solution)/shard_map/all_gather | solution.py:17
  239.0 39.5 %copy-start.22 = (f32[256]{0:T(256)S(1)}, f32[256]{0:T(256)}, u32[]{:S(2)}) copy-start(f32[256]{0:T(256)} %param.39) | copy-start | bytes 3076
  (3 other events, 6.4 us)
Sparse Core Ops, SparseCore 0:
  9.6 83.4 all-gather.2
  188.5 89.9 all-gather.4
where the time goes:
time: 330 us; the launch traced here: 329 us
  waiting for transfers between devices  162 us (49%)
  starting transfers between devices  39.7 us (12%)
  local copies, waits for them, and re-layouts  39.5 us (12%)
  blocking collectives  39.5 us (12%)
  other arithmetic  17.5 us (5%)
  matrix products  16.8 us (5%)
  between operations  14 us (4%)
    all_gather x2, waiting for transfers between devices, in_one_piece(): result = lax.all_gather(both, axis, axis=dim, tiled=True)  114 us
    all_to_all x3, waiting for transfers between devices, from_everyone(): return lax.all_to_all(copies, axis, split_axis=0, concat_axis=0, tiled=True)  48.2 us
    all_to_all x1, blocking collectives, summed_on_arrival(): parts = lax.all_to_all(split_up(array, dim, length), axis, 0, 0, tiled=True)  39.5 us
    all_to_all x3, starting transfers between devices, from_everyone(): return lax.all_to_all(copies, axis, split_axis=0, concat_axis=0, tiled=True)  27 us
    dynamic_update_slice x4, local copies, waits for them, and re-layouts, per_device(): lax.scan(partial(block_step, skip_gain), zero_memory, blocked)  17.5 us
    ppermute x4, starting transfers between devices, passed_along(): return lax.ppermute(array, axis, pairs)  12.5 us
    dot_general x7, matrix products, per_device(): jnp.dot(normed, piece, preferred_element_type=jnp.float32)  8.79 us
  transfers between devices with their start and end apart: 9, of which 4 were waited for; matrix products, arithmetic and copies ran while one was open for 18% of the time, Pallas kernels for 0%

commit v1 on v0

--- a/solution.py
+++ b/solution.py
@@ -3,12 +3,235 @@
 import jax
 import jax.numpy as jnp
 from jax import lax
+from jax.experimental import pallas as pl
+from jax.experimental.pallas import tpu as pltpu
 from jax.sharding import PartitionSpec as P
 
 HEAD_DIM = 64
 STATE = 128
 CM = 2048
 BLOCK = 128
+
+
+MESH = pl.DeviceIdType.MESH
+
+
+def gather_project_kernel(
+    n, offsets,
+    tok, gain, wi, ww, ws, wg, wr, wv, wsg, us, uf,
+    o_gate, o_inp, o_wr, o_rd, o_step, o_glu, o_us, o_uf,
+    normed, ap, aq, as_, bp, bq, cp, acc_a, acc_s, acc_b, acc_c,
+    local_sem, zs, zr, ys, yr,
+):
+    z = lax.axis_index("sp")
+    y = lax.axis_index("fs")
+    n_right, n_left = n // 2, (n - 1) // 2
+    z_next, z_prev = lax.rem(z + 1, n), lax.rem(z + n - 1, n)
+    y_next, y_prev = lax.rem(y + 1, 4), lax.rem(y + 3, 4)
+
+    pairs = [
+        (wi, ap.at[z]), (ww, aq.at[z]), (ws, as_.at[z]), (wg, bp.at[z]), (wr, bq.at[z]),
+        (wv, cp.at[z, :, pl.ds(0, 256)]), (wsg, cp.at[z, :, pl.ds(256, 256)]),
+        (us, o_us.at[z]), (uf, o_uf.at[z]),
+    ]
+    own = [pltpu.make_async_copy(s, d, local_sem.at[k]) for k, (s, d) in enumerate(pairs)]
+    for c in own:
+        c.start()
+    barrier = pltpu.get_barrier_semaphore()
+    for where in ({"sp": z_next}, {"sp": z_prev}, {"fs": y_next}, {"fs": y_prev}):
+        pl.semaphore_signal(barrier, inc=1, device_id=where, device_id_type=MESH)
+    for c in own:
+        c.wait()
+    pl.semaphore_wait(barrier, 4)
+
+    groups = [((ap,), (aq, as_)), ((bp,), (bq,)), ((cp,), ()), ((o_us,), (o_uf,))]
+    zbase, ybase, zi, yi = [], [], 0, 0
+    for two, one in groups:
+        zbase.append(zi)
+        ybase.append(yi)
+        zi += len(two) + len(one)
+        yi += len(two)
+
+    def shard(s, way):
+        return lax.rem(z + n - s, n) if way == 0 else lax.rem(z + s, n)
+
+    def part(buf, j, q):
+        rows = buf.shape[1] // 4
+        return buf.at[j, pl.ds(pl.multiple_of(q * rows, rows), rows)]
+
+    def z_copies(g, s, way):
+        two, one = groups[g]
+        j = shard(s - 1, way)
+        refs = [part(b, j, y) for b in two] + [b.at[j] for b in one]
+        where = {"sp": z_next if way == 0 else z_prev}
+        return [
+            pltpu.make_async_remote_copy(
+                src_ref=r, dst_ref=r, send_sem=zs.at[zbase[g] + k, way, s],
+                recv_sem=zr.at[zbase[g] + k, way, s], device_id=where, device_id_type=MESH)
+            for k, r in enumerate(refs)
+        ]
+
+    def z_arrivals(g, s, way):
+        two, one = groups[g]
+        j = shard(s, way)
+        refs = [part(b, j, y) for b in two] + [b.at[j] for b in one]
+        where = {"sp": z_next if way == 0 else z_prev}
+        return [
+            pltpu.make_async_remote_copy(
+                src_ref=r, dst_ref=r, send_sem=zs.at[zbase[g] + k, way, s],
+                recv_sem=zr.at[zbase[g] + k, way, s], device_id=where, device_id_type=MESH)
+            for k, r in enumerate(refs)
+        ]
+
+    def y_copy(g, s, way, kind, q):
+        j = shard(s, way)
+        up = kind == 0 or (kind == 2 and way == 0)
+        r = part(groups[g][0][0], j, q)
+        return pltpu.make_async_remote_copy(
+            src_ref=r, dst_ref=r, send_sem=ys.at[ybase[g], way, kind, s],
+            recv_sem=yr.at[ybase[g], way, kind, s],
+            device_id={"fs": y_next if up else y_prev}, device_id_type=MESH)
+
+    y_far = lax.rem(y + 2, 4)
+
+    def start_step(g, s, way):
+        for c in z_copies(g, s, way):
+            c.start()
+
+    def comm(g, s):
+        lasts = (n_right, n_left)
+        for way in (0, 1):
+            last = lasts[way]
+
+            @pl.when((s >= 1) & (s <= last))
+            def _():
+                for c in z_arrivals(g, s, way):
+                    c.wait_recv()
+
+            @pl.when(s < last)
+            def _():
+                start_step(g, s + 1, way)
+
+            if groups[g][0]:
+                @pl.when((s >= 1) & (s <= last))
+                def _():
+                    y_copy(g, s, way, 0, y).start()
+                    y_copy(g, s, way, 1, y).start()
+
+                @pl.when((s >= 2) & (s <= last + 1))
+                def _():
+                    y_copy(g, s - 1, way, 0, y_prev).wait_recv()
+                    y_copy(g, s - 1, way, 1, y_next).wait_recv()
+                    y_copy(g, s - 1, way, 2, y_prev if way == 0 else y_next).start()
+
+                @pl.when((s >= 3) & (s <= last + 2))
+                def _():
+                    y_copy(g, s - 2, way, 2, y_far).wait_recv()
+                    y_copy(g, s - 2, way, 0, y).wait_send()
+                    y_copy(g, s - 2, way, 1, y).wait_send()
+                    y_copy(g, s - 2, way, 2, y_prev if way == 0 else y_next).wait_send()
+
+            @pl.when((s >= 3) & (s <= last + 2))
+            def _():
+                for c in z_copies(g, s - 2, way):
+                    c.wait_send()
+
+    def both(ref, j1, j2, axis):
+        return jnp.concatenate([ref[j1], ref[j2]], axis=axis)
+
+    def multiply(g, s):
+        if g == 3:
+            return
+        lag = s - 2
+        j1 = jnp.where(lag == n_right, z, shard(lag, 0))
+        j2 = shard(lag, 1)
+        rows = both(normed, j1, j2, 1)
+        if g == 0:
+            w = jnp.concatenate([both(ap, j1, j2, 0), both(aq, j1, j2, 0)], axis=1)
+            acc_a[...] += jnp.dot(rows, w, preferred_element_type=jnp.float32)
+            acc_s[...] += lax.dot_general(
+                rows, both(as_, j1, j2, 1), (((1,), (1,)), ((), ())),
+                preferred_element_type=jnp.float32)
+        elif g == 1:
+            w = jnp.concatenate([both(bp, j1, j2, 0), both(bq, j1, j2, 0)], axis=1)
+            acc_b[...] += jnp.dot(rows, w, preferred_element_type=jnp.float32)
+        else:
+            acc_c[...] += jnp.dot(rows, both(cp, j1, j2, 0), preferred_element_type=jnp.float32)
+
+    for g in range(4):
+        if offsets[g] == 0:
+            start_step(g, 1, 0)
+            start_step(g, 1, 1)
+
+    def norm_rows(i, carry):
+        at = pl.ds(pl.multiple_of(i * 32, 32), 32)
+        x = tok[0, at, :].astype(jnp.float32)
+        scale = lax.rsqrt(jnp.mean(x * x, axis=-1, keepdims=True) + 1e-06)
+        x = (x * scale * gain[...]).astype(jnp.bfloat16)
+        for j in range(n):
+            normed[j, at, :] = x[:, j * 128:(j + 1) * 128]
+        return carry
+
+    lax.fori_loop(0, tok.shape[1] // 32, norm_rows, 0)
+    for acc in (acc_a, acc_s, acc_b, acc_c):
+        acc[...] = jnp.zeros_like(acc)
+
+    def slot(t, carry):
+        for g in range(4):
+            s = t - offsets[g]
+            low = 1 if offsets[g] == 0 else 0
+
+            @pl.when((s >= low) & (s <= n_right + 2))
+            def _():
+                comm(g, s)
+        for g in range(3):
+            s = t - offsets[g]
+
+            @pl.when((s >= 3) & (s <= n_right + 2))
+            def _():
+                multiply(g, s)
+        return carry
+
+    lax.fori_loop(1, n_right + 3 + max(offsets), slot, 0)
+    o_inp[...] = acc_a[:, :256].astype(jnp.bfloat16)
+    o_wr[...] = acc_a[:, 256:].astype(jnp.bfloat16)
+    o_step[...] = acc_s[...].astype(jnp.bfloat16)
+    o_gate[...] = acc_b[:, :256].astype(jnp.bfloat16)
+    o_rd[...] = acc_b[:, 256:].astype(jnp.bfloat16)
+    value = acc_c[:, :256].astype(jnp.bfloat16).astype(jnp.float32)
+    sig = acc_c[:, 256:].astype(jnp.bfloat16).astype(jnp.float32)
+    o_glu[...] = (value * jax.nn.sigmoid(sig)).astype(jnp.bfloat16)
+
+
+def gather_project(n, tokens, gain, wi, ww, wst, wg, wr, wv, wsg, us, uf):
+    t = tokens.shape[1]
+    f32, bf = jnp.float32, jnp.bfloat16
+    ws = jnp.pad(wst.T, ((0, 16 - wst.shape[1]), (0, 0)))
+    vm = pl.BlockSpec(memory_space=pltpu.VMEM)
+    hb = pl.BlockSpec(memory_space=pl.ANY)
+    out = lambda *s: jax.ShapeDtypeStruct(s, bf)
+    dma = pltpu.SemaphoreType.DMA
+    steps = n // 2 + 1
+    return pl.pallas_call(
+        partial(gather_project_kernel, n, (0, 1, 3, 5)),
+        out_shape=(out(t, 256), out(t, 256), out(t, 128), out(t, 128), out(t, 16), out(t, 256),
+                   out(n, 256, 128), out(n, 256, 128)),
+        in_specs=[vm, vm] + [hb] * 9,
+        out_specs=(vm,) * 8,
+        scratch_shapes=[
+            pltpu.VMEM((n, t, 128), bf),
+            pltpu.VMEM((n, 128, 256), bf), pltpu.VMEM((n, 128, 128), bf), pltpu.VMEM((n, 16, 128), bf),
+            pltpu.VMEM((n, 128, 256), bf), pltpu.VMEM((n, 128, 128), bf),
+            pltpu.VMEM((n, 128, 512), bf),
+            pltpu.VMEM((t, 384), f32), pltpu.VMEM((t, 16), f32), pltpu.VMEM((t, 384), f32),
+            pltpu.VMEM((t, 512), f32),
+            dma((9,)), dma((8, 2, steps)), dma((8, 2, steps)),
+            dma((4, 2, 3, steps)), dma((4, 2, 3, steps)),
+        ],
+        compiler_params=pltpu.CompilerParams(
+            collective_id=0, has_side_effects=True, vmem_limit_bytes=60 * 1024 * 1024),
+        name="gather_project",
+    )(tokens, gain.reshape(1, -1), wi, ww, ws, wg, wr, wv, wsg, us, uf)
 
 
 def in_one_piece(arrays, axis, dim, along):
@@ -119,31 +342,13 @@
     unproject_filter,
 ):
     row_count = tokens.shape[1]
-    source = tokens[0].astype(jnp.float32)
-    normed = (
-        source * lax.rsqrt(jnp.mean(source * source, axis=-1, keepdims=True) + 1e-06) * input_gain
-    ).astype(jnp.bfloat16)
-    pieces = in_one_piece(
-        (
-            weight_gate,
-            weight_input,
-            weight_write,
-            weight_read,
-            weight_step,
-            weight_value,
-            weight_sigmoid,
-        ),
-        "sp",
-        0,
-        1,
-    )
-    sums = tuple((jnp.dot(normed, piece, preferred_element_type=jnp.float32) for piece in pieces))
-    gate_values, input_values, write_values, read_values, step_values, value_rows, sigmoid_rows = (
-        total.astype(jnp.bfloat16) for total in sums
-    )
-    glu_rows = (
-        value_rows.astype(jnp.float32) * jax.nn.sigmoid(sigmoid_rows.astype(jnp.float32))
-    ).astype(jnp.bfloat16)
+    (gate_values, input_values, write_values, read_values, step_values, glu_rows, full_state,
+     full_filter) = gather_project(
+        lax.axis_size("sp"), tokens, input_gain, weight_input, weight_write, weight_step,
+        weight_gate, weight_read, weight_value, weight_sigmoid, unproject_state, unproject_filter)
+    step_values = step_values[:, : rate_log.shape[0]]
+    full_state = full_state.transpose(1, 0, 2).reshape(256, -1)
+    full_filter = full_filter.transpose(1, 0, 2).reshape(256, -1)
     short_rim = filter_input.shape[0] - 1
     long_rim = depth_filter.shape[0] - 1
     borders = passed_along(
@@ -214,7 +419,6 @@
         (filtered - mean_value[:, None]) * lax.rsqrt(variance + 1e-05)[:, None] * channel_gain
     )
     filter_out = jax.nn.silu(normal_rows).astype(jnp.bfloat16)
-    full_state, full_filter = in_one_piece((unproject_state, unproject_filter), "sp", 1, 0)
     summed = summed_on_arrival(
         (
             jnp.dot(state_out, full_state, preferred_element_type=jnp.float32)

time: 330 us -> 248 us (0.75)
  waiting for transfers between devices: 162 us -> 41.9 us
  Pallas kernels: 0 us -> 76.6 us
  between operations: 14 us -> 0.44 us
  matrix products: 16.8 us -> 6.74 us
  blocking collectives: 39.5 us -> 34 us
  other arithmetic: 17.5 us -> 13.1 us
  local copies, waits for them, and re-layouts: 39.5 us -> 35.3 us
    all_gather x2 -> x0, waiting for transfers between devices: 114 us -> none  [in_one_piece(): result = lax.all_gather(both, axis, axis=dim, tiled=True)]
    pallas_call x0 -> x1, Pallas kernels: none -> 76.6 us  [gather_project(): pl.pallas_call(partial(gather_project_kernel, n, (0, 1, 3, 5)), out_shape...]
    dot_general x7 -> x0, matrix products: 8.79 us -> none  [per_device(): jnp.dot(normed, piece, preferred_element_type=jnp.float32)]
    squeeze x8, local copies, waits for them, and re-layouts: 6.53 us -> 0.05 us  [per_device(): lax.scan(partial(block_step, skip_gain), zero_memory, blocked)]
    all_to_all x3, waiting for transfers between devices: 48.2 us -> 41.9 us  [from_everyone(): return lax.all_to_all(copies, axis, split_axis=0, concat_axis=0, tiled=True)]
    all_to_all x1, blocking collectives: 39.5 us -> 34 us  [summed_on_arrival(): parts = lax.all_to_all(split_up(array, dim, length), axis, 0, 0, tiled=True)]
  transfers between devices with their start and end apart: 9 -> 7, of which waited for: 4 -> 2; matrix products, arithmetic and copies ran while one was open for 18% -> 19% of each run, Pallas kernels for 0% -> 0%
where the time goes in v1:
time: 248 us; the launch traced here: 246 us
  Pallas kernels  76.6 us (31%)
  waiting for transfers between devices  41.9 us (17%)
  starting transfers between devices  38.2 us (15%)
  local copies, waits for them, and re-layouts  35.3 us (14%)
  blocking collectives  34 us (14%)
  other arithmetic  13.1 us (5%)
  matrix products  6.74 us (3%)
    pallas_call x1, Pallas kernels, gather_project(): pl.pallas_call(partial(gather_project_kernel, n, (0, 1, 3, 5)), out_shape...  76.6 us
    all_to_all x3, waiting for transfers between devices, from_everyone(): return lax.all_to_all(copies, axis, split_axis=0, concat_axis=0, tiled=True)  41.9 us
    all_to_all x1, blocking collectives, summed_on_arrival(): parts = lax.all_to_all(split_up(array, dim, length), axis, 0, 0, tiled=True)  34 us
    all_to_all x3, starting transfers between devices, from_everyone(): return lax.all_to_all(copies, axis, split_axis=0, concat_axis=0, tiled=True)  27.5 us
    dynamic_update_slice x4, local copies, waits for them, and re-layouts, per_device(): lax.scan(partial(block_step, skip_gain), zero_memory, blocked)  17.5 us
    ppermute x4, starting transfers between devices, passed_along(): return lax.ppermute(array, axis, pairs)  10.6 us
  transfers between devices with their start and end apart: 7, of which 2 were waited for; matrix products, arithmetic and copies ran while one was open for 19% of the time, Pallas kernels for 0%

profile of v1, /device:TPU:1, one launch (start us, length us, event | category | flops | bytes accessed | tf_op | source)
XLA Modules:
  0.0 246.3 jit_solution(13617863221533178782)
XLA Ops:
  0.0 1.3 pad.4.ws
  1.3 76.6 %gather_project.1 = (bf16[512,256]{1,0:T(8,128)(2,1)}, bf16[512,256]{1,0:T(8,128)(2,1)}, bf16[512,128]{1,0:T(8,128)(2,1)}, bf16[512,128]{1,0:T(8,128)(2,1)}, bf1...) custom-call(bf16[1,512,2048]{2,1,0:T(8,128)(2,1)} %tok.1, ...), custom_call_target="tpu_custom_call" | custom-call | tf_op jit(solution)/shard_map/gather_project/pallas_call | solution.py:215
  78.7 2.1 collective-permute-start.2
  81.4 2.5 %collective-permute-start.1 = (bf16[3,128]{1,0:T(4,128)(2,1)S(1)}, bf16[3,128]{1,0:T(4,128)(2,1)S(1)}, u32[]{:S(2)}, u32[]{:S(2)}) collective-permute-start(bf16[3,128]{1,0:T(4,128)(2,1)S(1)} %slice.305), channel_id=1, source_target_pairs={{0,32},{32,64},{64,96},{96,128},{128,160},{160,192},{192,224},{224... | collective-permute-start | bytes 2312 | tf_op jit(solution)/shard_map/ppermute | solution.py:247
  84.7 1.9 collective-permute-start
  87.3 4.1 %collective-permute-start.3 = (bf16[30,256]{1,0:T(8,128)(2,1)S(1)}, bf16[30,256]{1,0:T(8,128)(2,1)S(1)}, u32[]{:S(2)}, u32[]{:S(2)}) collective-permute-start(bf16[30,256]{1,0:T(8,128)(2,1)S(1)} %slice.327), channel_id=1, source_target_pairs={{0,32},{32,64},{64,96},{96,128},{128,160},{160,192},{192,224},{224... | collective-permute-start | bytes 46088 | tf_op jit(solution)/shard_map/ppermute | solution.py:247
  92.1 0.8 copy.142
  92.9 1.1 compare_select_fusion
  94.1 1.2 reduce-window.6
  96.6 7.2 %all-to-all-start = ((f32[16,1,4]{2,1,0:T(1,128)}), f32[16,1,4]{2,1,0:T(1,128)S(1)}, u32[]{:S(2)}, u32[]{:S(2)}) async-start(f32[16,1,4]{2,1,0:T(1,128)} %broadcast_in_dim.43), calls=%async_computation | async-start | bytes 16384 | tf_op jit(solution)/shard_map/all_to_all | solution.py:258
  104.0 0.9 maximum_convert_fusion.2
  105.2 1.0 maximum_convert_fusion.3
  107.6 2.9 %fusion.95 = (f32[512]{0:T(512)S(1)}, f32[512]{0:T(512)S(1)}, f32[512,256]{1,0:T(8,128)}) fusion(f32[542,256]{1,0:T(8,128)S(1)} %maximum_convert_fusion, f32[256]{0:T(256)S(1)} %bitcast.209, f32[256]{0:T(256)S(1)} %bitcast.208, f32[256]{0:T(256)S(1)} %bitcast.207, f32[256]{0:T(256)S(1)} %bitcast.206, f32[256]{0:T(256)S(1)} %bitcast.205, ...), kind=kLoop, calls=%fused_computation.183 | loop fusion | flops 8387584 | bytes 16813056 | tf_op jit(solution)/shard_map/reduce_sum | solution.py:414
  110.6 4.4 %all-to-all-done = f32[16,1,4]{2,1,0:T(1,128)S(1)} async-done(((f32[16,1,4]{2,1,0:T(1,128)}), f32[16,1,4]{2,1,0:T(1,128)S(1)}, u32[]{:S(2)}, u32[]{:S(2)}) %all-to-all-start) | async-done | bytes 288 | tf_op jit(solution)/shard_map/all_to_all | solution.py:258
  115.6 14.2 %all-to-all-start.2 = ((f32[8,1,1024]{2,1,0:T(1,128)}), f32[8,1,1024]{2,1,0:T(1,128)S(1)}, u32[]{:S(2)}, u32[]{:S(2)}) async-start(f32[8,1,1024]{2,1,0:T(1,128)} %broadcast_in_dim.47), calls=%async_computation.2 | async-start | bytes 65536 | tf_op jit(solution)/shard_map/all_to_all | solution.py:258
  129.8 22.4 %while.13 = (s32[]{:T(128)}, f32[4,64,128]{2,1,0:T(8,128)S(1)}, f32[4,128,4,64]{1,0,3,2:T(4,128)}, f32[4,128,4]{2,1,0:T(8,128)S(1)}, f32[4,128,4,64]{1,3,2,0:T(8...) while((s32[]{:T(128)}, f32[4,64,128]{2,1,0:T(8,128)S(1)}, ...), condition=%wide.region_2.3_spmd.clone, body=%wide.region_0.2_spmd.clone.sunk | while | flops 42696704 | bytes 1749232 | solution.py:388
  131.1 4.4 %dynamic_update_slice.6 = f32[4,128,4,64]{1,0,3,2:T(4,128)} dynamic-update-slice(f32[4,128,4,64]{1,0,3,2:T(4,128)} %get-tuple-element.315, f32[1,128,4,64]{1,0,3,2:T(1,128)S(1)} %bitcast.179, s32[]{:T(128)S(6)} %copy.191, s32[]{:T(128)} %constant.55.clone.1..sunk, s32[]{:T(128)} %constant.55.clone.1..sunk, s32[]{:T(128)} %constant.55.clone.1..sunk) | dynamic-update-slice | bytes 262148 | tf_op jit(solution)/shard_map/while/body/jit(dynamic_update_index_in_dim)/dynamic_update_slice | solution.py:388
  136.7 4.4 %dynamic_update_slice.6 = f32[4,128,4,64]{1,0,3,2:T(4,128)} dynamic-update-slice(f32[4,128,4,64]{1,0,3,2:T(4,128)} %get-tuple-element.315, f32[1,128,4,64]{1,0,3,2:T(1,128)S(1)} %bitcast.179, s32[]{:T(128)S(6)} %copy.191, s32[]{:T(128)} %constant.55.clone.1..sunk, s32[]{:T(128)} %constant.55.clone.1..sunk, s32[]{:T(128)} %constant.55.clone.1..sunk) | dynamic-update-slice | bytes 262148 | tf_op jit(solution)/shard_map/while/body/jit(dynamic_update_index_in_dim)/dynamic_update_slice | solution.py:388
  142.3 4.4 %dynamic_update_slice.6 = f32[4,128,4,64]{1,0,3,2:T(4,128)} dynamic-update-slice(f32[4,128,4,64]{1,0,3,2:T(4,128)} %get-tuple-element.315, f32[1,128,4,64]{1,0,3,2:T(1,128)S(1)} %bitcast.179, s32[]{:T(128)S(6)} %copy.191, s32[]{:T(128)} %constant.55.clone.1..sunk, s32[]{:T(128)} %constant.55.clone.1..sunk, s32[]{:T(128)} %constant.55.clone.1..sunk) | dynamic-update-slice | bytes 262148 | tf_op jit(solution)/shard_map/while/body/jit(dynamic_update_index_in_dim)/dynamic_update_slice | solution.py:388
  147.9 4.4 %dynamic_update_slice.6 = f32[4,128,4,64]{1,0,3,2:T(4,128)} dynamic-update-slice(f32[4,128,4,64]{1,0,3,2:T(4,128)} %get-tuple-element.315, f32[1,128,4,64]{1,0,3,2:T(1,128)S(1)} %bitcast.179, s32[]{:T(128)S(6)} %copy.191, s32[]{:T(128)} %constant.55.clone.1..sunk, s32[]{:T(128)} %constant.55.clone.1..sunk, s32[]{:T(128)} %constant.55.clone.1..sunk) | dynamic-update-slice | bytes 262148 | tf_op jit(solution)/shard_map/while/body/jit(dynamic_update_index_in_dim)/dynamic_update_slice | solution.py:388
  152.3 1.3 broadcast_in_dim.46
  153.5 6.2 %all-to-all-start.1 = ((bf16[16,1,4,64,128]{4,3,2,1,0:T(8,128)(2,1)}), bf16[16,1,4,64,128]{4,3,2,1,0:T(8,128)(2,1)S(1)}, u32[]{:S(2)}, u32[]{:S(2)}) async-start(bf16[16,1,4,64,128]{4,3,2,1,0:T(8,128)(2,1)} %broadcast_in_dim.46), calls=%async_computation.1 | async-start | bytes 2097152 | tf_op jit(solution)/shard_map/all_to_all | solution.py:258
  159.7 1.5 copy.154
  161.3 1.5 copy.156
  166.7 2.0 reshape.137
  168.7 0.8 reduce_sum.51
  169.6 37.4 %all-to-all-done.1 = bf16[16,1,4,64,128]{4,3,2,1,0:T(8,128)(2,1)S(1)} async-done(((bf16[16,1,4,64,128]{4,3,2,1,0:T(8,128)(2,1)}), bf16[16,1,4,64,128]{4,3,2,1,0:T(8,128)(2,1)S(1)}, u32[]{:S(2)}, u32[]{:S(2)}) %all-to-all-start.1) | async-done | bytes 1048608 | tf_op jit(solution)/shard_map/all_to_all | solution.py:258
  207.7 1.5 fusion.32
  209.6 0.8 fusion.73
  210.5 0.8 add_convert_fusion
  211.3 34.0 %all_to_all.21 = bf16[8,64,2048]{2,1,0:T(8,128)(2,1)S(1)} all-to-all(bf16[8,64,2048]{2,1,0:T(8,128)(2,1)S(1)} %bitcast.175), channel_id=1, replica_groups=mesh['sp'=16,'fs'=4,'tp'=8] {'tp'}, dimensions={0} | all-to-all | bytes 4194304 | tf_op jit(solution)/shard_map/all_to_all | solution.py:284
  245.2 1.1 reduce_sum.52
  (126 shorter events, 17.1 us)
Async XLA Ops:
  0.0 103.7 %copy-start.5 = (bf16[31,256]{1,0:T(8,128)(2,1)S(1)}, bf16[31,256]{1,0:T(8,128)(2,1)}, u32[]{:S(2)}) copy-start(bf16[31,256]{1,0:T(8,128)(2,1)} %param.42) | copy-start | bytes 47620
  0.0 103.8 %copy-start.8 = (bf16[4,128]{1,0:T(4,128)(2,1)S(1)}, bf16[4,128]{1,0:T(4,128)(2,1)}, u32[]{:S(2)}) copy-start(bf16[4,128]{1,0:T(4,128)(2,1)} %param.34) | copy-start | bytes 3076
  0.0 103.8 %copy-start.9 = (bf16[4,128]{1,0:T(4,128)(2,1)S(1)}, bf16[4,128]{1,0:T(4,128)(2,1)}, u32[]{:S(2)}) copy-start(bf16[4,128]{1,0:T(4,128)(2,1)} %param.35) | copy-start | bytes 3076
  0.0 103.8 %copy-start.6 = (bf16[4,256]{1,0:T(4,128)(2,1)S(1)}, bf16[4,256]{1,0:T(4,128)(2,1)}, u32[]{:S(2)}) copy-start(bf16[4,256]{1,0:T(4,128)(2,1)} %param.33) | copy-start | bytes 6148
  77.9 28.4 %copy-start.3 = (bf16[512,256]{1,0:T(8,128)(2,1)S(1)}, bf16[512,256]{1,0:T(8,128)(2,1)}, u32[]{:S(2)}) copy-start(bf16[512,256]{1,0:T(8,128)(2,1)} %get-tuple-element.62) | copy-start | bytes 786436
  78.7 26.5 %collective-permute-start.2 = (bf16[3,128]{1,0:T(4,128)(2,1)S(1)}, bf16[3,128]{1,0:T(4,128)(2,1)S(1)}, u32[]{:S(2)}, u32[]{:S(2)}) collective-permute-start(bf16[3,128]{1,0:T(4,128)(2,1)S(1)} %slice.314), channel_id=1, source_target_pairs={{0,32},{32,64},{64,96},{96,128},{128,160},{160,192},{192,224},{224... | collective-permute-start | bytes 2312 | tf_op jit(solution)/shard_map/ppermute | solution.py:247
  81.4 22.6 %collective-permute-start.1 = (bf16[3,128]{1,0:T(4,128)(2,1)S(1)}, bf16[3,128]{1,0:T(4,128)(2,1)S(1)}, u32[]{:S(2)}, u32[]{:S(2)}) collective-permute-start(bf16[3,128]{1,0:T(4,128)(2,1)S(1)} %slice.305), channel_id=1, source_target_pairs={{0,32},{32,64},{64,96},{96,128},{128,160},{160,192},{192,224},{224... | collective-permute-start | bytes 2312 | tf_op jit(solution)/shard_map/ppermute | solution.py:247
  84.7 21.7 %collective-permute-start = (bf16[3,256]{1,0:T(4,128)(2,1)S(1)}, bf16[3,256]{1,0:T(4,128)(2,1)S(1)}, u32[]{:S(2)}, u32[]{:S(2)}) collective-permute-start(bf16[3,256]{1,0:T(4,128)(2,1)S(1)} %slice.296), channel_id=1, source_target_pairs={{0,32},{32,64},{64,96},{96,128},{128,160},{160,192},{192,224},{224... | collective-permute-start | bytes 4616 | tf_op jit(solution)/shard_map/ppermute | solution.py:247
  87.3 20.2 %collective-permute-start.3 = (bf16[30,256]{1,0:T(8,128)(2,1)S(1)}, bf16[30,256]{1,0:T(8,128)(2,1)S(1)}, u32[]{:S(2)}, u32[]{:S(2)}) collective-permute-start(bf16[30,256]{1,0:T(8,128)(2,1)S(1)} %slice.327), channel_id=1, source_target_pairs={{0,32},{32,64},{64,96},{96,128},{128,160},{160,192},{192,224},{224... | collective-permute-start | bytes 46088 | tf_op jit(solution)/shard_map/ppermute | solution.py:247
  96.6 18.4 %all-to-all-start = ((f32[16,1,4]{2,1,0:T(1,128)}), f32[16,1,4]{2,1,0:T(1,128)S(1)}, u32[]{:S(2)}, u32[]{:S(2)}) async-start(f32[16,1,4]{2,1,0:T(1,128)} %broadcast_in_dim.43), calls=%async_computation | async-start | bytes 16384 | tf_op jit(solution)/shard_map/all_to_all | solution.py:258
  105.2 2.4 copy-start.2
  107.6 22.2 %copy-start.11 = (f32[4]{0:T(128)S(1)}, f32[4]{0:T(128)}, u32[]{:S(2)}) copy-start(f32[4]{0:T(128)} %param.38) | copy-start | bytes 52
  115.6 36.6 %all-to-all-start.2 = ((f32[8,1,1024]{2,1,0:T(1,128)}), f32[8,1,1024]{2,1,0:T(1,128)S(1)}, u32[]{:S(2)}, u32[]{:S(2)}) async-start(f32[8,1,1024]{2,1,0:T(1,128)} %broadcast_in_dim.47), calls=%async_computation.2 | async-start | bytes 65536 | tf_op jit(solution)/shard_map/all_to_all | solution.py:258
  152.3 7.5 %copy-start.4 = (f32[8,1,1024]{2,1,0:T(1,128)}, f32[8,1,1024]{2,1,0:T(1,128)S(1)}, u32[]{:S(2)}) copy-start(f32[8,1,1024]{2,1,0:T(1,128)S(1)} %all-to-all-done.2) | copy-start | bytes 98308
  153.5 53.5 %all-to-all-start.1 = ((bf16[16,1,4,64,128]{4,3,2,1,0:T(8,128)(2,1)}), bf16[16,1,4,64,128]{4,3,2,1,0:T(8,128)(2,1)S(1)}, u32[]{:S(2)}, u32[]{:S(2)}) async-start(bf16[16,1,4,64,128]{4,3,2,1,0:T(8,128)(2,1)} %broadcast_in_dim.46), calls=%async_computation.1 | async-start | bytes 2097152 | tf_op jit(solution)/shard_map/all_to_all | solution.py:258
  159.7 49.6 %copy-start.1 = (bf16[512,256]{1,0:T(8,128)(2,1)S(1)}, bf16[512,256]{1,0:T(8,128)(2,1)}, u32[]{:S(2)}) copy-start(bf16[512,256]{1,0:T(8,128)(2,1)} %get-tuple-element.67) | copy-start | bytes 786436
  169.5 40.1 %copy-start.7 = (f32[256]{0:T(256)S(1)}, f32[256]{0:T(256)}, u32[]{:S(2)}) copy-start(f32[256]{0:T(256)} %param.39) | copy-start | bytes 3076
  209.1 1.3 copy-start.10
  209.4 1.1 copy-start

commit v2 on v0

v2 whole, which is shorter than its diff:
```python
from functools import partial

import jax
import jax.numpy as jnp
from jax import lax
from jax.experimental import pallas as pl
from jax.experimental.pallas import tpu as pltpu
from jax.sharding import PartitionSpec as P

MESH = pl.DeviceIdType.MESH
F32, BF16 = jnp.float32, jnp.bfloat16
CHANNELS = 2048
OFFSETS = (0, 1, 3, 5)
AFTER = 2


def mixer_kernel(
    n,
    tok, gain, wi, ww, ws, wg, wr, wv, wsg, us, uf,
    f_in, f_wr, f_rd, bias, rate, skip, out_gain, opening, shift, taps, ch_gain,
    out,
    normed, ap, aq, as_, bp, bq, cp, up, uq, acc_a, acc_s, acc_b, acc_c,
    halo_src, halo_dst, glu_src, glu_dst, ext4, ext31, x_ref, b_ref, c_ref, gate_ref,
    rows_ref, cols_ref, inside, filtered, stat, ebuf, tbuf, e_right, e_left, run, act,
    pbuf, d2d_src, d2d_dst, far_src, far_dst, rn_src, rn_dst, dn_src, dn_dst,
    local_sem, zs, zr, ys, yr, es, er, hs, hr, ss, sr, os_, or_,
):
    z = lax.axis_index("sp")
    y = lax.axis_index("fs")
    tp = lax.axis_index("tp")
    x, core = tp // 2, lax.rem(tp, 2)
    n_right, n_left = n // 2, (n - 1) // 2
    z_next, z_prev = lax.rem(z + 1, n), lax.rem(z + n - 1, n)
    y_next, y_prev = lax.rem(y + 1, 4), lax.rem(y + 3, 4)
    t_rows = tok.shape[1]

    pairs = [
        (wi, ap.at[z]), (ww, aq.at[z]), (ws, as_.at[z]), (wg, bp.at[z]), (wr, bq.at[z]),
        (wv, cp.at[z, :, pl.ds(0, 256)]), (wsg, cp.at[z, :, pl.ds(256, 256)]),
        (us, up.at[z]), (uf, uq.at[z]),
    ]
    own = [pltpu.make_async_copy(s, d, local_sem.at[k]) for k, (s, d) in enumerate(pairs)]
    for c in own:
        c.start()
    barrier = pltpu.get_barrier_semaphore()
    greet = [{"sp": z_next}, {"sp": z_prev}, {"fs": y_next}, {"fs": y_prev}]
    greet += [{"tp": lax.rem(tp + i, 8)} for i in range(1, 8)]
    for where in greet:
        pl.semaphore_signal(barrier, inc=1, device_id=where, device_id_type=MESH)
    for c in own:
        c.wait()
    pl.semaphore_wait(barrier, len(greet))

    def remote(src, dst, send, recv, where):
        return pltpu.make_async_remote_copy(
            src_ref=src, dst_ref=dst, send_sem=send, recv_sem=recv, device_id=where,
            device_id_type=MESH)

    groups = [((ap,), (aq, as_)), ((bp,), (bq,)), ((cp,), ()), ((up,), (uq,))]
    zbase, zi = [], 0
    for two, one in groups:
        zbase.append(zi)
        zi += len(two) + len(one)

    def shard(s, way):
        return lax.rem(z + n - s, n) if way == 0 else lax.rem(z + s, n)

    def part(buf, j, q):
        rows = buf.shape[1] // 4
        return buf.at[j, pl.ds(pl.multiple_of(q * rows, rows), rows)]

    def z_copies(g, s, way, j):
        two, one = groups[g]
        refs = [part(b, j, y) for b in two] + [b.at[j] for b in one]
        where = {"sp": z_next if way == 0 else z_prev}
        return [
            remote(r, r, zs.at[zbase[g] + k, way, s], zr.at[zbase[g] + k, way, s], where)
            for k, r in enumerate(refs)
        ]

    def y_copy(g, s, way, kind, q):
        up_way = kind == 0 or (kind == 2 and way == 0)
        r = part(groups[g][0][0], shard(s, way), q)
        return remote(r, r, ys.at[g, way, kind, s], yr.at[g, way, kind, s],
                      {"fs": y_next if up_way else y_prev})

    y_far = lax.rem(y + 2, 4)

    def start_step(g, s, way):
        for c in z_copies(g, s, way, shard(s - 1, way)):
            c.start()

    def comm(g, s):
        for way in (0, 1):
            last = (n_right, n_left)[way]

            @pl.when((s >= 1) & (s <= last))
            def _():
                for c in z_copies(g, s, way, shard(s, way)):
                    c.wait_recv()

            @pl.when(s < last)
            def _():
                start_step(g, s + 1, way)

            @pl.when((s >= 1) & (s <= last))
            def _():
                y_copy(g, s, way, 0, y).start()
                y_copy(g, s, way, 1, y).start()

            @pl.when((s >= 2) & (s <= last + 1))
            def _():
                y_copy(g, s - 1, way, 0, y_prev).wait_recv()
                y_copy(g, s - 1, way, 1, y_next).wait_recv()
                y_copy(g, s - 1, way, 2, y_prev if way == 0 else y_next).start()

            @pl.when((s >= 3) & (s <= last + 2))
            def _():
                y_copy(g, s - 2, way, 2, y_far).wait_recv()
                y_copy(g, s - 2, way, 0, y).wait_send()
                y_copy(g, s - 2, way, 1, y).wait_send()
                y_copy(g, s - 2, way, 2, y_prev if way == 0 else y_next).wait_send()
                for c in z_copies(g, s - 2, way, shard(s - 3, way)):
                    c.wait_send()

    def both(ref, j1, j2, axis):
        return jnp.concatenate([ref[j1], ref[j2]], axis=axis)

    def multiply(g, s):
        lag = s - 2
        j1 = jnp.where(lag == n_right, z, shard(lag, 0))
        j2 = shard(lag, 1)
        rows = both(normed, j1, j2, 1)
        if g == 0:
            w = jnp.concatenate([both(ap, j1, j2, 0), both(aq, j1, j2, 0)], axis=1)
            acc_a[...] += jnp.dot(rows, w, preferred_element_type=F32)
            acc_s[:, :16] += lax.dot_general(
                rows, both(as_, j1, j2, 1), (((1,), (1,)), ((), ())),
                preferred_element_type=F32)
        elif g == 1:
            w = jnp.concatenate([both(bp, j1, j2, 0), both(bq, j1, j2, 0)], axis=1)
            acc_b[...] += jnp.dot(rows, w, preferred_element_type=F32)
        else:
            acc_c[...] += jnp.dot(rows, both(cp, j1, j2, 0), preferred_element_type=F32)

    def border(k):
        src, dst = [
            (halo_src.at[:, pl.ds(0, 384)], halo_dst.at[:, pl.ds(0, 384)]),
            (halo_src.at[:, pl.ds(384, 128)], halo_dst.at[:, pl.ds(384, 128)]),
            (glu_src, glu_dst),
        ][k]
        return remote(src, dst, hs.at[k], hr.at[k], {"sp": z_next})

    def short_filter(lo, hi, kernel, target):
        weights = [kernel[k:k + 1, :].astype(F32) for k in range(4)]

        def strip(i, carry):
            block = ext4[pl.ds(pl.multiple_of(i * 64, 64), 72), lo:hi]
            total = weights[0] * pltpu.roll(block, 72 - 5, 0)[:64]
            for k in range(1, 4):
                total = total + weights[k] * pltpu.roll(block, 72 - 5 - k, 0)[:64]
            target[pl.ds(pl.multiple_of(i * 64, 64), 64), :] = (
                total * jax.nn.sigmoid(total)).astype(BF16)
            return carry

        lax.fori_loop(0, t_rows // 64, strip, 0)

    def take_border(k, lo, hi):
        border(k).wait_recv()
        rows = halo_dst[:, lo:hi].astype(F32)[8:]
        ext4[0:8, lo:hi] = jnp.where(z > 0, rows, 0.0)

    def finish_a():
        mapped = acc_a[...].astype(BF16)
        halo_src[:, 0:384] = mapped[t_rows - 16:]
        ext4[8:, 0:384] = mapped.astype(F32)
        border(0).start()

    def finish_b():
        mapped = acc_b[...].astype(BF16)
        halo_src[:, 384:512] = mapped[t_rows - 16:, 256:]
        ext4[8:, 384:512] = mapped[:, 256:].astype(F32)
        border(1).start()
        gate_ref[...] = mapped[:, :256]

    def finish_c():
        value = acc_c[:, :256].astype(BF16).astype(F32)
        sig = acc_c[:, 256:].astype(BF16).astype(F32)
        glu = (value * jax.nn.sigmoid(sig)).astype(BF16)
        glu_src[...] = glu[t_rows - 32:]
        border(2).start()
        ext31[32:, :] = glu.astype(F32)

    lane = lax.broadcasted_iota(jnp.int32, (1, 128), 1)

    def by_head(first, rows=slice(None)):
        c = cols_ref[rows, first:first + 4]
        return jnp.concatenate(
            [jnp.where(lane < 64, c[:, 2 * k:2 * k + 1], c[:, 2 * k + 1:2 * k + 2])
             for k in range(2)], axis=1)

    def local_state():
        take_border(0, 0, 384)
        short_filter(0, 256, f_in, x_ref)
        short_filter(256, 384, f_wr, b_ref)
        head = lax.broadcasted_iota(jnp.int32, (8, t_rows), 0)
        place = lax.broadcasted_iota(jnp.int32, (8, t_rows), 1)
        bias8 = jnp.zeros((8, t_rows), F32)
        rate8 = jnp.zeros((8, t_rows), F32)
        for h in range(4):
            bias8 = jnp.where(head == h, bias[h], bias8)
            rate8 = jnp.where(head == h, rate[h], rate8)
        steps = acc_s[...].astype(BF16).astype(F32).T[:8] + bias8
        steps = jnp.maximum(steps, 0.0) + jnp.log1p(jnp.exp(-jnp.abs(steps)))
        rows_ref[0:4, :] = shift[0]
        rows_ref[4:8, :] = jnp.zeros((4, t_rows), F32)
        total = rows_ref[0:8, :] - steps * jnp.exp(rate8)
        k = 1
        while k < t_rows:
            total = total + jnp.where(place >= k, pltpu.roll(total, k, 1), 0.0)
            k *= 2
        end = total[:, t_rows - 1:t_rows]
        rows_ref[0:8, :] = total
        rows_ref[8:16, :] = steps
        rows_ref[16:24, :] = steps * jnp.exp(end - total)
        rows_ref[24:32, :] = jnp.exp(total)
        rows_ref[32:, :] = jnp.zeros((96, t_rows), F32)
        cols_ref[...] = rows_ref[...].T
        scaled = (x_ref[...].astype(F32) * by_head(16)).astype(BF16)
        ebuf[z] = lax.dot_general(
            b_ref[...], scaled, (((0,), (0,)), ((), ())), preferred_element_type=F32
        ).astype(BF16)
        spread = jnp.concatenate(
            [jnp.where(lane < 64, end[2 * k:2 * k + 1, :], end[2 * k + 1:2 * k + 2, :])
             for k in range(2)], axis=1)
        tbuf[z] = jnp.broadcast_to(spread, (8, 256))
        e_right[...] = jnp.zeros_like(e_right)
        run[...] = jnp.zeros_like(run)
        e_left[...] = opening[0].reshape(256, 128).T

    def e_copies(s, way, j):
        where = {"sp": z_next if way == 0 else z_prev}
        return [remote(r.at[j], r.at[j], es.at[k, way, s], er.at[k, way, s], where)
                for k, r in enumerate((ebuf, tbuf))]

    def state_ring(s):
        for way in (0, 1):
            last = (n_right, n_left)[way]

            @pl.when((s >= 1) & (s <= last))
            def _():
                for c in e_copies(s, way, shard(s, way)):
                    c.wait_recv()

            @pl.when(s < last)
            def _():
                for c in e_copies(s + 1, way, shard(s, way)):
                    c.start()

            @pl.when((s >= 1) & (s <= last))
            def _():
                for c in e_copies(s, way, shard(s - 1, way)):
                    c.wait_send()
                j = shard(s, way)
                total = tbuf[j][0:1]
                if way == 0:
                    @pl.when(z >= s)
                    def _():
                        e_right[...] += jnp.exp(run[0:1, :]) * ebuf[j].astype(F32)
                        run[...] += total
                else:
                    @pl.when(z + s >= n)
                    def _():
                        e_left[...] = e_left[...] * jnp.exp(total) + ebuf[j].astype(F32)

    def inside_strip(i):
        k = 128 * (i + 1)
        at = slice(128 * i, k)
        scores = lax.dot_general(
            c_ref[at, :], b_ref[0:k, :], (((1,), (1,)), ((), ())), preferred_element_type=F32)
        diag = (lax.broadcasted_iota(jnp.int32, (128, k), 0) + 128 * i
                >= lax.broadcasted_iota(jnp.int32, (128, k), 1))
        pieces = []
        for h in range(4):
            gap = cols_ref[at, h:h + 1] - rows_ref[h:h + 1, 0:k]
            decay = jnp.exp(jnp.where(diag, gap, -jnp.inf)) * rows_ref[8 + h:9 + h, 0:k]
            tile = slice(128 * (h // 2), 128 * (h // 2) + 128)
            pieces.append(jnp.dot((scores * decay).astype(BF16), x_ref[0:k, tile],
                                  preferred_element_type=F32))
        for k in range(2):
            gains = jnp.where(lane < 64, skip[2 * k], skip[2 * k + 1])
            lanes = slice(128 * k, 128 * k + 128)
            inside[at, lanes] = (jnp.where(lane < 64, pieces[2 * k], pieces[2 * k + 1])
                                 + gains * x_ref[at, lanes].astype(F32))

    def stat_copy(i, to):
        slot = tp if to else lax.rem(tp + 8 - i, 8)
        return remote(stat.at[slot], stat.at[slot], ss.at[i], sr.at[i],
                      {"tp": lax.rem(tp + i, 8)})

    def long_filter():
        border(2).wait_recv()
        ext31[0:32, :] = jnp.where(z > 0, glu_dst[...].astype(F32), 0.0)

        def strip(i, carry):
            block = ext31[pl.ds(pl.multiple_of(i * 32, 32), 64), :]
            total = jnp.zeros((32, 256), F32)
            for r in range(8):
                moved = block if r == 0 else pltpu.roll(block, 64 - r, 0)
                for a in range(5):
                    k = 8 * a + r - 2
                    if 0 <= k < 31 and 8 * a + 32 <= 64:
                        total = total + taps[k:k + 1, :].astype(F32) * moved[8 * a:8 * a + 32]
            at = pl.ds(pl.multiple_of(i * 32, 32), 32)
            filtered[at, :] = total
            inside_sums = jnp.concatenate(
                [jnp.sum(total, axis=1, keepdims=True),
                 jnp.sum(total * total, axis=1, keepdims=True)], axis=1)
            cols_ref[at, 64:66] = inside_sums
            return carry

        lax.fori_loop(0, t_rows // 32, strip, 0)
        stat[tp] = cols_ref[...].T[64:72]
        for i in range(1, 8):
            stat_copy(i, True).start()

    def filter_act():
        for i in range(1, 8):
            stat_copy(i, False).wait_recv()
        sums = stat[0]
        for i in range(1, 8):
            sums = sums + stat[i]
        mean = sums[0:1] / CHANNELS
        var = sums[1:2] / CHANNELS - mean * mean
        scale = lax.rsqrt(var + 1e-05)
        rows_ref[32:33, :] = mean
        rows_ref[33:34, :] = scale
        back = rows_ref[...].T

        def strip(i, carry):
            at = pl.ds(pl.multiple_of(i * 64, 64), 64)
            f = (filtered[at, :] - cols_ref[at, 32:33]) * cols_ref[at, 33:34] * ch_gain[...]
            act[at, 256:512] = (f * jax.nn.sigmoid(f)).astype(BF16)
            return carry

        cols_ref[:, 32:34] = back[:, 32:34]
        lax.fori_loop(0, t_rows // 64, strip, 0)
        for i in range(1, 8):
            stat_copy(i, True).wait_send()

    for g in range(4):
        if OFFSETS[g] == 0:
            start_step(g, 1, 0)
            start_step(g, 1, 1)

    def norm_rows(i, carry):
        at = pl.ds(pl.multiple_of(i * 32, 32), 32)
        v = tok[0, at, :].astype(F32)
        scale = lax.rsqrt(jnp.mean(v * v, axis=-1, keepdims=True) + 1e-06)
        v = (v * scale * gain[...]).astype(BF16)
        for j in range(n):
            normed[j, at, :] = v[:, j * 128:(j + 1) * 128]
        return carry

    lax.fori_loop(0, t_rows // 32, norm_rows, 0)
    for acc in (acc_a, acc_s, acc_b, acc_c):
        acc[...] = jnp.zeros_like(acc)

    done = [n_right + 2 + o for o in OFFSETS]
    state_at = done[0] + AFTER
    read_at = max(done[1] + AFTER, state_at + 1)
    long_at = done[2] + AFTER
    last_slot = max(max(done), state_at + n_right, read_at + 4, long_at + 4) + 1

    def slot(t, carry):
        for g in range(4):
            s = t - OFFSETS[g]
            low = 1 if OFFSETS[g] == 0 else 0

            @pl.when((s >= low) & (s <= n_right + 2))
            def _():
                comm(g, s)

        @pl.when((t > state_at) & (t <= state_at + n_right))
        def _():
            state_ring(t - state_at)

        for g in range(3):
            s = t - OFFSETS[g]

            @pl.when((s >= 3) & (s <= n_right + 2))
            def _():
                multiply(g, s)

        @pl.when(t == done[0])
        def _():
            finish_a()

        @pl.when(t == done[1])
        def _():
            finish_b()

        @pl.when(t == done[2])
        def _():
            finish_c()

        @pl.when(t == state_at)
        def _():
            local_state()
            for way in (0, 1):
                for c in e_copies(1, way, z):
                    c.start()

        @pl.when(t == long_at)
        def _():
            long_filter()

        @pl.when(t == read_at)
        def _():
            take_border(1, 384, 512)
            short_filter(384, 512, f_rd, c_ref)

        for i in range(4):
            @pl.when(t == read_at + 1 + i)
            def _():
                inside_strip(i)

        @pl.when(t == long_at + 3)
        def _():
            filter_act()
        return carry

    lax.fori_loop(1, last_slot, slot, 0)
    for k in range(3):
        border(k).wait_send()

    entering = (e_left[...] * jnp.exp(run[0:1, :]) + e_right[...]).astype(BF16)
    for i in range(4):
        at = slice(128 * i, 128 * i + 128)
        carried = jnp.dot(c_ref[at, :], entering, preferred_element_type=F32)
        v = inside[at, :] + by_head(24, at) * carried
        g = gate_ref[at, :].astype(F32)
        v = v * (g * jax.nn.sigmoid(g))
        v = v * lax.rsqrt(jnp.mean(v * v, axis=-1, keepdims=True) + 1e-06)
        act[at, 0:256] = (v * out_gain[...]).astype(BF16)

    blocks = CHANNELS // 256

    def rows_of(xx, cc):
        return pl.ds(pl.multiple_of((2 * xx + cc) * 64, 64), 64)

    def at_x(k):
        return {"tp": 2 * lax.rem(x + k, 4) + core}

    def pair_copy(b):
        return remote(d2d_src.at[b], d2d_dst.at[b], os_.at[0, b], or_.at[0, b],
                      {"tp": 2 * x + 1 - core})

    def far_copy(b):
        return remote(far_src.at[b], far_dst.at[b], os_.at[1, b], or_.at[1, b],
                      at_x(1 + 2 * lax.rem(b, 2)))

    def relay_copy(b):
        return remote(rn_src.at[b], rn_dst.at[b], os_.at[2, b], or_.at[2, b],
                      at_x(1 + 2 * lax.rem(b, 2)))

    def direct_copy(b):
        return remote(dn_src.at[b], dn_dst.at[b], os_.at[3, b], or_.at[3, b],
                      at_x(3 + 2 * lax.rem(b, 2)))

    def stage_multiply(b):
        w = jnp.concatenate(
            [jnp.concatenate([ref[2 * b], ref[2 * b + 1]], axis=1) for ref in (up, uq)], axis=0)
        pbuf[b] = jnp.dot(act[...], w, preferred_element_type=F32)
        for xx in range(4):
            d2d_src[b, xx] = pbuf[b, rows_of(xx, 1 - core), :].astype(BF16)
        pair_copy(b).start()

    def stage_pair(b):
        pair_copy(b).wait_recv()
        for xx in range(4):
            at = rows_of(xx, core)
            pbuf[b, at, :] = pbuf[b, at, :] + d2d_dst[b, xx].astype(F32)
        far_src[b] = pbuf[b, rows_of(lax.rem(x + 2, 4), core), :].astype(BF16)
        far_copy(b).start()
        dn_src[b] = pbuf[b, rows_of(lax.rem(x + 3 + 2 * lax.rem(b, 2), 4), core), :].astype(BF16)
        direct_copy(b).start()

    def stage_relay(b):
        far_copy(b).wait_recv()
        mine = pbuf[b, rows_of(lax.rem(x + 1 + 2 * lax.rem(b, 2), 4), core), :]
        rn_src[b] = (mine + far_dst[b].astype(F32)).astype(BF16)
        relay_copy(b).start()

    def stage_out(b):
        relay_copy(b).wait_recv()
        direct_copy(b).wait_recv()
        total = (pbuf[b, rows_of(x, core), :] + rn_dst[b].astype(F32)) + dn_dst[b].astype(F32)
        out[0, :, pl.ds(pl.multiple_of(b * 256, 256), 256)] = total.astype(BF16)
        for c in (pair_copy(b), far_copy(b), relay_copy(b), direct_copy(b)):
            c.wait_send()

    def out_slot(i, carry):
        @pl.when(i < blocks)
        def _():
            stage_multiply(i)

        for lag, stage in ((2, stage_pair), (5, stage_relay), (8, stage_out)):
            @pl.when((i >= lag) & (i < blocks + lag))
            def _():
                stage(i - lag)
        return carry

    lax.fori_loop(0, blocks + 8, out_slot, 0)


def per_device(
    tokens, input_gain, weight_gate, weight_input, weight_write, weight_read, weight_step,
    weight_value, weight_sigmoid, filter_input, filter_write, filter_read, step_bias, rate_log,
    skip_gain, output_gain, opening_state, decay_shift, depth_filter, channel_gain,
    unproject_state, unproject_filter,
):
    n = lax.axis_size("sp")
    t = tokens.shape[1]
    ws = jnp.pad(weight_step.T, ((0, 16 - weight_step.shape[1]), (0, 0)))
    vm = pl.BlockSpec(memory_space=pltpu.VMEM)
    sm = pl.BlockSpec(memory_space=pltpu.SMEM)
    hb = pl.BlockSpec(memory_space=pl.ANY)
    dma = pltpu.SemaphoreType.DMA
    steps = n // 2 + 1
    v = pltpu.VMEM
    return pl.pallas_call(
        partial(mixer_kernel, n),
        out_shape=jax.ShapeDtypeStruct((1, t // 8, CHANNELS), BF16),
        in_specs=[vm, vm] + [hb] * 9 + [vm] * 3 + [sm] * 3 + [vm] * 5,
        out_specs=vm,
        scratch_shapes=[
            v((n, t, 128), BF16),
            v((n, 128, 256), BF16), v((n, 128, 128), BF16), v((n, 16, 128), BF16),
            v((n, 128, 256), BF16), v((n, 128, 128), BF16), v((n, 128, 512), BF16),
            v((n, 256, 128), BF16), v((n, 256, 128), BF16),
            v((t, 384), F32), v((t, 128), F32), v((t, 384), F32), v((t, 512), F32),
            v((16, 512), BF16), v((16, 512), BF16), v((32, 256), BF16), v((32, 256), BF16),
            v((8 + t, 512), F32), v((32 + t, 256), F32),
            v((t, 256), BF16), v((t, 128), BF16), v((t, 128), BF16), v((t, 256), BF16),
            v((128, t), F32), v((t, 128), F32), v((t, 256), F32), v((t, 256), F32),
            v((8, 8, t), F32), v((n, 128, 256), BF16), v((n, 8, 256), F32),
            v((128, 256), F32), v((128, 256), F32), v((8, 256), F32), v((t, 512), BF16),
            v((8, t, 256), F32), v((8, 4, 64, 256), BF16), v((8, 4, 64, 256), BF16),
            *[v((8, 64, 256), BF16)] * 6,
            dma((9,)), dma((8, 2, steps)), dma((8, 2, steps)),
            dma((4, 2, 3, steps)), dma((4, 2, 3, steps)),
            dma((2, 2, steps)), dma((2, 2, steps)), dma((3,)), dma((3,)),
            dma((8,)), dma((8,)), dma((4, 8)), dma((4, 8)),
        ],
        compiler_params=pltpu.CompilerParams(
            collective_id=0, has_side_effects=True, vmem_limit_bytes=62 * 1024 * 1024),
        name="mixer",
    )(
        tokens, input_gain.reshape(1, -1), weight_input, weight_write, ws, weight_gate,
        weight_read, weight_value, weight_sigmoid, unproject_state, unproject_filter,
        filter_input, filter_write, filter_read, step_bias, rate_log, skip_gain,
        output_gain.reshape(1, -1), opening_state, decay_shift, depth_filter,
        channel_gain.reshape(1, -1),
    )


def solution(mesh):
    in_specs = (
        P("fs", "sp", None),
        P(),
        P("sp", "tp"),
        P("sp", "tp"),
        P("sp", "tp"),
        P("sp", "tp"),
        P("sp", "tp"),
        P("sp", "tp"),
        P("sp", "tp"),
        P(None, "tp"),
        P(None, "tp"),
        P(None, "tp"),
        P("tp"),
        P("tp"),
        P("tp"),
        P("tp"),
        P("fs", "tp", None, None),
        P("fs", "tp", "sp"),
        P(None, "tp"),
        P("tp"),
        P("tp", "sp"),
        P("tp", "sp"),
    )
    out_specs = P("fs", ("sp", "tp"), None)
    return jax.shard_map(
        per_device, mesh=mesh, in_specs=in_specs, out_specs=out_specs, check_vma=False
    )
```

time: 330 us -> 127 us (0.38)
  waiting for transfers between devices: 162 us -> 0 us
  Pallas kernels: 0 us -> 123 us
  starting transfers between devices: 39.7 us -> 0 us
  blocking collectives: 39.5 us -> 0 us
  local copies, waits for them, and re-layouts: 39.5 us -> 2.95 us
  other arithmetic: 17.5 us -> 0 us
  matrix products: 16.8 us -> 0 us
  between operations: 14 us -> 0.01 us
    pallas_call x0 -> x1, Pallas kernels: none -> 123 us  [per_device(): pl.pallas_call(partial(mixer_kernel, n), out_shape=jax.ShapeDtypeStruct((...]
    all_gather x2 -> x0, waiting for transfers between devices: 114 us -> none  [in_one_piece(): result = lax.all_gather(both, axis, axis=dim, tiled=True)]
    all_to_all x3 -> x0, waiting for transfers between devices: 48.2 us -> none  [from_everyone(): return lax.all_to_all(copies, axis, split_axis=0, concat_axis=0, tiled=True)]
    all_to_all x1 -> x0, blocking collectives: 39.5 us -> none  [summed_on_arrival(): parts = lax.all_to_all(split_up(array, dim, length), axis, 0, 0, tiled=True)]
    all_to_all x3 -> x0, starting transfers between devices: 27 us -> none  [from_everyone(): return lax.all_to_all(copies, axis, split_axis=0, concat_axis=0, tiled=True)]
    dynamic_update_slice x4 -> x0, local copies, waits for them, and re-layouts: 17.5 us -> none  [per_device(): lax.scan(partial(block_step, skip_gain), zero_memory, blocked)]
    dot_general x23 -> x0, matrix products: 16.8 us -> none  [the longest x7 8.79 us: per_device(): jnp.dot(normed, piece, preferred_element_type=jnp.float32)]
    ppermute x4 -> x0, starting transfers between devices: 12.5 us -> none  [passed_along(): return lax.ppermute(array, axis, pairs)]
  transfers between devices with their start and end apart: 9 -> 0, of which waited for: 4 -> 0; matrix products, arithmetic and copies ran while one was open for 18% -> 0% of each run, Pallas kernels for 0% -> 0%
where the time goes in v2:
time: 127 us; the launch traced here: 126 us
  Pallas kernels  123 us (97%)
  local copies, waits for them, and re-layouts  2.95 us (2%)
    pallas_call x1, Pallas kernels, per_device(): pl.pallas_call(partial(mixer_kernel, n), out_shape=jax.ShapeDtypeStruct((...  123 us

profile of v2, /device:TPU:1, one launch (start us, length us, event | category | flops | bytes accessed | tf_op | source)
XLA Modules:
  0.0 126.4 jit_solution(15149454885099209870)
XLA Ops:
  0.0 1.3 %pad.4.ws = bf16[16,128]{1,0:T(8,128)(2,1)} pad(bf16[4,128]{1,0:T(4,128)(2,1)} %bitcast.7, bf16[]{:T(256)} %constant.2.clone.1), padding=0_12x0_0 | pad | bytes 5122 | tf_op jit(solution)/shard_map/jit(_pad)/pad | solution.py:525
  1.3 123.5 %mixer.1 = bf16[1,64,2048]{2,1,0:T(8,128)(2,1)} custom-call(bf16[1,512,2048]{2,1,0:T(8,128)(2,1)} %tok.1, f32[1,2048]{1,0:T(1,128)} %bitcast.4, bf16[128,256]{1,0:T(8,128)(2,1)} %wi.1, bf16[128,128]{1,0:T(8,128)(2,1)} %ww.1, bf16[16,128]{1,0:T(8,128)(2,1)} %pad.4.ws, bf16[128,256]{1,0:T(8,128)(2,1)} %wg.1, bf16[128,128]{1,0:T(8,128)(2,1)} %wr.1, ...), custom_call_target="tpu_custom_call" | custom-call | tf_op jit(solution)/shard_map/mixer/pallas_call | solution.py:532
  124.7 1.7 %copy.24 = bf16[1,64,2048]{2,1,0:T(8,128)(2,1)} copy(bf16[1,64,2048]{2,1,0:T(8,128)(2,1)} %mixer.1) | data formatting | bytes 524288

commit v3 on v2

v3 whole, which is shorter than its diff:
```python
from functools import partial

import jax
import jax.numpy as jnp
from jax import lax
from jax.experimental import pallas as pl
from jax.experimental.pallas import tpu as pltpu
from jax.sharding import PartitionSpec as P

MESH = pl.DeviceIdType.MESH
F32, BF16 = jnp.float32, jnp.bfloat16
CHANNELS = 2048
OFFSETS = (0, 1, 8)
LONG_TO_ACT = 3


def mixer_kernel(
    n,
    tok_h, gain_h, wi, ww, ws_h, wg, wr, wv, wsg, us, uf,
    f_in_h, f_wr_h, f_rd_h, bias_h, rate_h, skip_h, out_gain_h, opening_h, shift_h, taps_h,
    ch_gain_h,
    out,
    tok, gain, ws_v, f_in, f_wr, f_rd, bias, rate, skip, out_gain, opening, shift, taps, ch_gain,
    normed, ap, aq, as_, cp, cq, up, acc_a, acc_s, acc_c, blank, tapsb,
    tok_edge, ext4, ext31, x_ref, b_ref, c_ref, gate_ref,
    rows_ref, cols_ref, inside, filtered, sums_ref, stat, ebuf, tbuf, e_right, e_left, run, act,
    pbuf, d2d_src, d2d_dst, far_src, far_dst, rn_src, rn_dst, dn_src, dn_dst,
    local_sem, zs, zr, ys, yr, es, er, hs, hr, ss, sr, os_, or_,
):
    z = lax.axis_index("sp")
    y = lax.axis_index("fs")
    tp = lax.axis_index("tp")
    x, core = tp // 2, lax.rem(tp, 2)
    n_right, n_left = n // 2, (n - 1) // 2
    z_next, z_prev = lax.rem(z + 1, n), lax.rem(z + n - 1, n)
    y_next, y_prev = lax.rem(y + 1, 4), lax.rem(y + 3, 4)
    t_rows = tok.shape[0]

    barrier = pltpu.get_barrier_semaphore()
    greet = [{"sp": z_next}, {"sp": z_prev}, {"fs": y_next}, {"fs": y_prev}]
    greet += [{"tp": lax.rem(tp + i, 8)} for i in range(1, 8)]
    for where in greet:
        pl.semaphore_signal(barrier, inc=1, device_id=where, device_id_type=MESH)

    pairs = [
        (ws_h, ws_v), (wi, ap.at[z, :, pl.ds(0, 256)]), (wg, ap.at[z, :, pl.ds(256, 256)]),
        (ww, aq.at[z, :, pl.ds(0, 128)]), (wr, aq.at[z, :, pl.ds(128, 128)]),
        (tok_h.at[0], tok), (gain_h, gain), (wv, cp.at[z, :, pl.ds(0, 256)]),
        (wsg.at[:, pl.ds(0, 128)], cp.at[z, :, pl.ds(256, 128)]),
        (wsg.at[:, pl.ds(128, 128)], cq.at[z]),
        (us, up.at[z, pl.ds(0, 256)]), (uf, up.at[z, pl.ds(256, 256)]),
        (f_in_h, f_in), (f_wr_h, f_wr), (f_rd_h, f_rd), (bias_h, bias), (rate_h, rate),
        (skip_h, skip), (out_gain_h, out_gain), (opening_h.at[0], opening),
        (shift_h.at[0], shift), (taps_h, taps), (ch_gain_h, ch_gain),
    ]
    own = [pltpu.make_async_copy(s, d, local_sem.at[k]) for k, (s, d) in enumerate(pairs)]
    for c in own:
        c.start()

    def remote(src, dst, send, recv, where):
        return pltpu.make_async_remote_copy(
            src_ref=src, dst_ref=dst, send_sem=send, recv_sem=recv, device_id=where,
            device_id_type=MESH)

    def wait_bytes(sem, count):
        ref = blank.at[pl.ds(0, count // 512)]
        pltpu.make_async_copy(ref, ref, sem).wait()

    groups = [(ap, (aq, as_)), (cp, (cq,)), (up, ())]
    part_bytes = [ref.shape[1] // 4 * ref.shape[2] * 2 for ref, _ in groups]
    z_bytes = [p + sum(ref.shape[1] * ref.shape[2] * 2 for ref in one)
               for p, (_, one) in zip(part_bytes, groups)]

    def shard(s, way):
        return lax.rem(z + n - s, n) if way == 0 else lax.rem(z + s, n)

    def part(buf, j, q):
        rows = buf.shape[1] // 4
        return buf.at[j, pl.ds(pl.multiple_of(q * rows, rows), rows)]

    def pieces(g, c, j):
        two, one = groups[g]
        if c == 0:
            return [part(two, j, y)]
        rows = one[0].shape[1] // 2
        more = [b.at[j] for b in one[1:]] if c == 2 else []
        return [one[0].at[j, pl.ds((c - 1) * rows, rows)]] + more

    chunks = [3 if one else 1 for _, one in groups]
    first = [sum(chunks[:g]) for g in range(len(groups))]

    def chunk_bytes(g, c):
        if c == 0:
            return part_bytes[g]
        one = groups[g][1]
        rest = sum(r.shape[1] * r.shape[2] * 2 for r in one[1:]) if c == 2 else 0
        return one[0].shape[1] * one[0].shape[2] + rest

    def start_chunk(g, c, s, way):
        for r in pieces(g, c, shard(s - 1, way)):
            remote(r, r, zs.at[g, way, lax.rem(s, 4)], zr.at[first[g] + c, way, s - 1],
                   {"sp": z_next if way == 0 else z_prev}).start()

    y_far = lax.rem(y + 2, 4)
    direct_from = n_right - 1

    def y_start(g, s, way, kind, q):
        up_way = kind == 0 or (kind == 2 and way == 0)
        r = part(groups[g][0], shard(s, way), q)
        k = kind // 2
        where = y_far if kind == 3 else (y_next if up_way else y_prev)
        remote(r, r, ys.at[g, k, lax.rem(s, 4)], yr.at[g, k, s - 1], {"fs": where}).start()

    def y_wait(sem, g, s, per_way):
        @pl.when(s <= n_left)
        def _():
            wait_bytes(sem, 2 * per_way * part_bytes[g])

        @pl.when(s > n_left)
        def _():
            wait_bytes(sem, per_way * part_bytes[g])

    def comm(g, s):
        for c in range(chunks[g]):
            for way in (0, 1):
                last = (n_right, n_left)[way]

                @pl.when((s >= 1) & (s <= last))
                def _():
                    wait_bytes(zr.at[first[g] + c, way, s - 1], chunk_bytes(g, c))

                @pl.when(s < last)
                def _():
                    start_chunk(g, c, s + 1, way)

                if c == 0:
                    @pl.when((s >= 1) & (s <= last))
                    def _():
                        y_start(g, s, way, 0, y)
                        y_start(g, s, way, 1, y)

                        @pl.when(s >= direct_from)
                        def _():
                            y_start(g, s, way, 3, y)

        @pl.when((s >= 3) & (s <= n_right + 2))
        def _():
            wait_bytes(zs.at[g, 0, lax.rem(s - 2, 4)], z_bytes[g])

            @pl.when(s - 2 <= n_left)
            def _():
                wait_bytes(zs.at[g, 1, lax.rem(s - 2, 4)], z_bytes[g])

    def share(g, s):
        @pl.when((s >= 2) & (s <= n_right + 1))
        def _():
            y_wait(yr.at[g, 0, s - 2], g, s - 1, 2)

            @pl.when(s - 1 < direct_from)
            def _():
                y_start(g, s - 1, 0, 2, y_prev)
                y_start(g, s - 1, 1, 2, y_next)

        def complete(k, carry):
            y_wait(yr.at[g, 1, k - 1], g, k, 1)
            y_wait(ys.at[g, 0, lax.rem(k, 4)], g, k, 2)
            y_wait(ys.at[g, 1, lax.rem(k, 4)], g, k, 1)
            if g < 2:
                with jax.named_scope("mm"):
                    multiply(g, k)
            return carry

        @pl.when((s >= 4) & (s <= n_right + 2))
        def _():
            low = jnp.where(s > n_right + 1, s - 2, s - 3)
            high = jnp.where(s > n_right, s - 2, s - 3)
            lax.fori_loop(low, high + 1, complete, 0)

    def both(ref, j1, j2, axis):
        return jnp.concatenate([ref[j1], ref[j2]], axis=axis)

    def multiply(g, k):
        j1 = jnp.where(k == n_right, z, shard(k, 0))
        j2 = shard(k, 1)
        rows = both(normed, j1, j2, 1)
        if g == 0:
            w = jnp.concatenate([both(ap, j1, j2, 0), both(aq, j1, j2, 0)], axis=1)
            acc_a[...] += jnp.dot(rows, w, preferred_element_type=F32)
            acc_s[:, :16] += lax.dot_general(
                rows, both(as_, j1, j2, 1), (((1,), (1,)), ((), ())),
                preferred_element_type=F32)
        else:
            w = jnp.concatenate([both(cp, j1, j2, 0), both(cq, j1, j2, 0)], axis=1)
            acc_c[...] += jnp.dot(rows, w, preferred_element_type=F32)

    edge_lanes = pl.ds(pl.multiple_of(tp * 256, 256), 256)

    def border():
        return remote(tok.at[pl.ds(t_rows - 32, 32), edge_lanes], tok_edge.at[:, edge_lanes],
                      hs.at[0], hr.at[0], {"sp": z_next})

    def border_share(i):
        ref = tok_edge.at[:, edge_lanes]
        return remote(ref, ref, hs.at[1], hr.at[1], {"tp": lax.rem(tp + i, 8)})

    def short_filter(lo, hi, kernel, target):
        weights = [kernel[k:k + 1, :].astype(F32) for k in range(4)]

        def strip(i, carry):
            block = ext4[pl.ds(pl.multiple_of(i * 64, 64), 72), lo:hi]
            total = weights[0] * pltpu.roll(block, 72 - 5, 0)[:64]
            for k in range(1, 4):
                total = total + weights[k] * pltpu.roll(block, 72 - 5 - k, 0)[:64]
            target[pl.ds(pl.multiple_of(i * 64, 64), 64), :] = (
                total * jax.nn.sigmoid(total)).astype(BF16)
            return carry

        lax.fori_loop(0, t_rows // 64, strip, 0)

    def finish_a():
        mapped = acc_a[...].astype(BF16)
        own_rows = mapped[:t_rows]
        edge = jnp.where(z > 0, acc_a[t_rows + 24:, :].astype(BF16).astype(F32), 0.0)
        ext4[0:8, 0:256] = edge[:, 0:256]
        ext4[0:8, 256:512] = edge[:, 512:768]
        ext4[8:, 0:256] = own_rows[:, 0:256].astype(F32)
        ext4[8:, 256:512] = own_rows[:, 512:768].astype(F32)
        gate_ref[...] = own_rows[:, 256:512]

    def finish_c():
        value = acc_c[:, :256].astype(BF16).astype(F32)
        sig = acc_c[:, 256:].astype(BF16).astype(F32)
        glu = (value * jax.nn.sigmoid(sig)).astype(BF16).astype(F32)
        ext31[0:32, :] = jnp.where(z > 0, glu[t_rows:], 0.0)
        ext31[32:, :] = glu[:t_rows]

    lane = lax.broadcasted_iota(jnp.int32, (1, 128), 1)

    def by_head(first, rows=slice(None)):
        c = cols_ref[rows, first:first + 4]
        return jnp.concatenate(
            [jnp.where(lane < 64, c[:, 2 * k:2 * k + 1], c[:, 2 * k + 1:2 * k + 2])
             for k in range(2)], axis=1)

    def local_state():
        short_filter(0, 256, f_in, x_ref)
        short_filter(256, 384, f_wr, b_ref)
        head = lax.broadcasted_iota(jnp.int32, (8, t_rows), 0)
        place = lax.broadcasted_iota(jnp.int32, (8, t_rows), 1)
        bias8 = jnp.zeros((8, t_rows), F32)
        rate8 = jnp.zeros((8, t_rows), F32)
        for h in range(4):
            bias8 = jnp.where(head == h, bias[h], bias8)
            rate8 = jnp.where(head == h, rate[h], rate8)
        steps = acc_s[0:t_rows, :].astype(BF16).astype(F32).T[:8] + bias8
        steps = jnp.maximum(steps, 0.0) + jnp.log1p(jnp.exp(-jnp.abs(steps)))
        rows_ref[0:4, :] = shift[...]
        rows_ref[4:8, :] = jnp.zeros((4, t_rows), F32)
        total = rows_ref[0:8, :] - steps * jnp.exp(rate8)
        k = 1
        while k < t_rows:
            total = total + jnp.where(place >= k, pltpu.roll(total, k, 1), 0.0)
            k *= 2
        end = total[:, t_rows - 1:t_rows]
        rows_ref[0:8, :] = total
        rows_ref[8:16, :] = steps
        rows_ref[16:24, :] = steps * jnp.exp(end - total)
        rows_ref[24:32, :] = jnp.exp(total)
        rows_ref[32:, :] = jnp.zeros((96, t_rows), F32)
        cols_ref[...] = rows_ref[...].T
        scaled = (x_ref[...].astype(F32) * by_head(16)).astype(BF16)
        ebuf[z] = lax.dot_general(
            b_ref[...], scaled, (((0,), (0,)), ((), ())), preferred_element_type=F32
        ).astype(BF16)
        spread = jnp.concatenate(
            [jnp.where(lane < 64, end[2 * k:2 * k + 1, :], end[2 * k + 1:2 * k + 2, :])
             for k in range(2)], axis=1)
        tbuf[z] = jnp.broadcast_to(spread, (8, 256))

    e_bytes = (2 * 32 * 256,) * 3 + (2 * 32 * 256 + 4 * 8 * 256,)

    def state_start(c, s, way):
        j = shard(s - 1, way)
        where = {"sp": z_next if way == 0 else z_prev}
        for r in [ebuf.at[j, pl.ds(32 * c, 32)]] + [tbuf.at[j]] * (c // 3):
            remote(r, r, es.at[way, lax.rem(s, 2)], er.at[c, way, s - 1], where).start()

    def state_ring(s):
        for c in range(4):
            for way in (0, 1):
                last = (n_right, n_left)[way]

                @pl.when(s <= last)
                def _():
                    wait_bytes(er.at[c, way, s - 1], e_bytes[c])

                @pl.when(s < last)
                def _():
                    state_start(c, s + 1, way)

        for way in (0, 1):
            last = (n_right, n_left)[way]

            @pl.when(s <= last)
            def _():
                j = shard(s, way)
                total = tbuf[j][0:1]
                if way == 0:
                    @pl.when(z >= s)
                    def _():
                        e_right[...] += jnp.exp(run[0:1, :]) * ebuf[j].astype(F32)
                        run[...] += total
                else:
                    @pl.when(z + s >= n)
                    def _():
                        e_left[...] = e_left[...] * jnp.exp(total) + ebuf[j].astype(F32)
                wait_bytes(es.at[way, lax.rem(s, 2)], sum(e_bytes))

    def inside_strip(i):
        k = 128 * (i + 1)
        at = slice(128 * i, k)
        scores = lax.dot_general(
            c_ref[at, :], b_ref[0:k, :], (((1,), (1,)), ((), ())), preferred_element_type=F32)
        diag = (lax.broadcasted_iota(jnp.int32, (128, k), 0) + 128 * i
                >= lax.broadcasted_iota(jnp.int32, (128, k), 1))
        pieces = []
        for h in range(4):
            gap = cols_ref[at, h:h + 1] - rows_ref[h:h + 1, 0:k]
            decay = jnp.exp(jnp.where(diag, gap, -jnp.inf)) * rows_ref[8 + h:9 + h, 0:k]
            tile = slice(128 * (h // 2), 128 * (h // 2) + 128)
            pieces.append(jnp.dot((scores * decay).astype(BF16), x_ref[0:k, tile],
                                  preferred_element_type=F32))
        for k in range(2):
            gains = jnp.where(lane < 64, skip[2 * k], skip[2 * k + 1])
            lanes = slice(128 * k, 128 * k + 128)
            inside[at, lanes] = (jnp.where(lane < 64, pieces[2 * k], pieces[2 * k + 1])
                                 + gains * x_ref[at, lanes].astype(F32))

    def stat_copy(i):
        return remote(stat.at[tp], stat.at[tp], ss.at[0], sr.at[0], {"tp": lax.rem(tp + i, 8)})

    def long_filter(half):
        def strip(i, carry):
            block = ext31[pl.ds(pl.multiple_of(i * 64, 64), 96), :]
            total = jnp.zeros((8, 8, 256), F32)
            for r in range(8):
                moved = block if r == 0 else pltpu.roll(block, 96 - r, 0)
                for a in range(5):
                    k = 8 * a + r - 2
                    if 0 <= k < 31:
                        total = total + (tapsb[8 * k:8 * k + 8, :][None]
                                         * moved[8 * a:8 * a + 64].reshape(8, 8, 256))
            total = total.reshape(64, 256)
            at = pl.ds(pl.multiple_of(i * 64, 64), 64)
            filtered[at, :] = total
            sum1 = jnp.sum(total, axis=1, keepdims=True)
            sum2 = jnp.sum(total * total, axis=1, keepdims=True)
            sums_ref[at, :] = jnp.where(lane == 0, sum1, jnp.where(lane == 1, sum2, 0.0))
            return carry

        lax.fori_loop(half * (t_rows // 128), (half + 1) * (t_rows // 128), strip, 0)

    def send_sums():
        stat[tp] = sums_ref[...].T[0:8]
        for i in range(1, 8):
            stat_copy(i).start()

    def filter_act():
        with jax.named_scope("fact_wait"):
            wait_bytes(sr.at[0], 7 * 8 * t_rows * 4)
        sums = stat[0]
        for i in range(1, 8):
            sums = sums + stat[i]
        mean = sums[0:1] / CHANNELS
        var = sums[1:2] / CHANNELS - mean * mean
        rows_ref[32:33, :] = mean
        rows_ref[33:34, :] = lax.rsqrt(var + 1e-05)
        sums_ref[...] = rows_ref[...].T

        def strip(i, carry):
            at = pl.ds(pl.multiple_of(i * 64, 64), 64)
            f = (filtered[at, :] - sums_ref[at, 32:33]) * sums_ref[at, 33:34] * ch_gain[...]
            act[at, 256:512] = (f * jax.nn.sigmoid(f)).astype(BF16)
            return carry

        lax.fori_loop(0, t_rows // 64, strip, 0)
        wait_bytes(ss.at[0], 7 * 8 * t_rows * 4)

    own[0].wait()
    as_[z] = jnp.concatenate([ws_v[...].astype(F32), jnp.zeros((12, 128), F32)]).astype(BF16)
    for c in own[1:5]:
        c.wait()
    with jax.named_scope("entry"):
        pl.semaphore_wait(barrier, len(greet))
    for c in range(chunks[0]):
        start_chunk(0, c, 1, 0)
        start_chunk(0, c, 1, 1)
    for c in own[5:]:
        c.wait()

    border().start()

    def norm_rows(source, at, to):
        v = source[at, :].astype(F32)
        scale = lax.rsqrt(jnp.mean(v * v, axis=-1, keepdims=True) + 1e-06)
        v = (v * scale * gain[...]).astype(BF16)
        for j in range(n):
            normed[j, to, :] = v[:, j * 128:(j + 1) * 128]

    def norm_strip(i, carry):
        at = pl.ds(pl.multiple_of(i * 32, 32), 32)
        norm_rows(tok, at, at)
        return carry

    with jax.named_scope("norm"):
        lax.fori_loop(0, t_rows // 32, norm_strip, 0)
    e_right[...] = jnp.zeros_like(e_right)
    run[...] = jnp.zeros_like(run)
    e_left[...] = opening[...].reshape(256, 128).T
    for acc in (acc_a, acc_s, acc_c):
        acc[...] = jnp.zeros_like(acc)
    for k in range(taps.shape[0]):
        tapsb[8 * k:8 * k + 8, :] = jnp.broadcast_to(
            taps[k:k + 1, :].astype(F32), (8, 256))

    done = [n_right + 2 + o for o in OFFSETS]
    state_at = done[0]
    long_at = done[1] + 1
    acts_at = long_at + LONG_TO_ACT
    last_slot = max(max(done), state_at + n_right, state_at + 5, acts_at) + 1

    def slot(t, carry):
        @pl.when((t > state_at) & (t <= state_at + n_right))
        def _():
            with jax.named_scope("ring"):
                state_ring(t - state_at)

        for g in range(3):
            s = t - OFFSETS[g]
            low = 1 if g == 0 else 0

            @pl.when((s >= low) & (s <= n_right + 2))
            def _():
                with jax.named_scope("comm%d" % g):
                    comm(g, s)

        @pl.when(t == 1)
        def _():
            border().wait_recv()
            for i in range(1, 8):
                border_share(i).start()

        @pl.when(t == 3)
        def _():
            wait_bytes(hr.at[1], 7 * 32 * 256 * 2)
            norm_rows(tok_edge, pl.ds(0, 32), pl.ds(t_rows, 32))

        for g in range(3):
            s = t - OFFSETS[g]

            @pl.when((s >= 2) & (s <= n_right + 2))
            def _():
                with jax.named_scope("share%d" % g):
                    share(g, s)

        @pl.when(t == state_at)
        def _():
            with jax.named_scope("lstate"):
                finish_a()
                local_state()
            for c in range(4):
                for way in (0, 1):
                    state_start(c, 1, way)

        @pl.when(t == done[1])
        def _():
            with jax.named_scope("fin_c"):
                finish_c()

        @pl.when(t == state_at + 1)
        def _():
            with jax.named_scope("read"):
                short_filter(384, 512, f_rd, c_ref)

        for i in range(4):
            @pl.when(t == state_at + 2 + i)
            def _():
                with jax.named_scope("inside"):
                    inside_strip(i)

        @pl.when(t == long_at)
        def _():
            with jax.named_scope("longf"):
                long_filter(0)

        @pl.when(t == long_at + 1)
        def _():
            with jax.named_scope("longf"):
                long_filter(1)
                send_sums()

        @pl.when(t == acts_at)
        def _():
            with jax.named_scope("fact"):
                filter_act()
        return carry

    lax.fori_loop(1, last_slot, slot, 0)
    border().wait_send()
    wait_bytes(hs.at[1], 7 * 32 * 256 * 2)

    entering = (e_left[...] * jnp.exp(run[0:1, :]) + e_right[...]).astype(BF16)
    for i in range(4):
        at = slice(128 * i, 128 * i + 128)
        carried = jnp.dot(c_ref[at, :], entering, preferred_element_type=F32)
        v = inside[at, :] + by_head(24, at) * carried
        g = gate_ref[at, :].astype(F32)
        v = v * (g * jax.nn.sigmoid(g))
        v = v * lax.rsqrt(jnp.mean(v * v, axis=-1, keepdims=True) + 1e-06)
        act[at, 0:256] = (v * out_gain[...]).astype(BF16)

    blocks = CHANNELS // 256

    def rows_of(xx, cc):
        return pl.ds(pl.multiple_of((2 * xx + cc) * 64, 64), 64)

    def at_x(k):
        return {"tp": 2 * lax.rem(x + k, 4) + core}

    def pair_copy(b):
        return remote(d2d_src.at[b], d2d_dst.at[b], os_.at[0], or_.at[0, b],
                      {"tp": 2 * x + 1 - core})

    def far_copy(b):
        return remote(far_src.at[b], far_dst.at[b], os_.at[1], or_.at[1, b],
                      at_x(1 + 2 * lax.rem(b, 2)))

    def relay_copy(b):
        return remote(rn_src.at[b], rn_dst.at[b], os_.at[2], or_.at[2, b],
                      at_x(1 + 2 * lax.rem(b, 2)))

    def direct_copy(b):
        return remote(dn_src.at[b], dn_dst.at[b], os_.at[3], or_.at[3, b],
                      at_x(3 + 2 * lax.rem(b, 2)))

    def stage_multiply(b):
        w = both(up, 2 * b, 2 * b + 1, 1)
        pbuf[b] = jnp.dot(act[...], w, preferred_element_type=F32)
        for xx in range(4):
            d2d_src[b, xx] = pbuf[b, rows_of(xx, 1 - core), :].astype(BF16)
        pair_copy(b).start()

    def stage_pair(b):
        pair_copy(b).wait_recv()
        for xx in range(4):
            at = rows_of(xx, core)
            pbuf[b, at, :] = pbuf[b, at, :] + d2d_dst[b, xx].astype(F32)
        far_src[b] = pbuf[b, rows_of(lax.rem(x + 2, 4), core), :].astype(BF16)
        far_copy(b).start()

    def stage_direct(b):
        dn_src[b] = pbuf[b, rows_of(lax.rem(x + 3 + 2 * lax.rem(b, 2), 4), core), :].astype(BF16)
        direct_copy(b).start()

    def stage_relay(b):
        far_copy(b).wait_recv()
        mine = pbuf[b, rows_of(lax.rem(x + 1 + 2 * lax.rem(b, 2), 4), core), :]
        rn_src[b] = (mine + far_dst[b].astype(F32)).astype(BF16)
        relay_copy(b).start()

    def stage_out(b):
        relay_copy(b).wait_recv()
        direct_copy(b).wait_recv()
        total = (pbuf[b, rows_of(x, core), :] + rn_dst[b].astype(F32)) + dn_dst[b].astype(F32)
        out[0, :, pl.ds(pl.multiple_of(b * 256, 256), 256)] = total.astype(BF16)

    def out_slot(i, carry):
        @pl.when(i < blocks)
        def _():
            with jax.named_scope("o_mm"):
                stage_multiply(i)

        for lag, stage in ((2, stage_pair), (5, stage_relay), (6, stage_direct), (9, stage_out)):
            @pl.when((i >= lag) & (i < blocks + lag))
            def _():
                with jax.named_scope("o_st%d" % lag):
                    stage(i - lag)
        return carry

    lax.fori_loop(0, blocks + 9, out_slot, 0)
    with jax.named_scope("o_end"):
        for k, r in enumerate((d2d_src, far_src, rn_src, dn_src)):
            pltpu.make_async_copy(r, r, os_.at[k]).wait()


def per_device(
    tokens, input_gain, weight_gate, weight_input, weight_write, weight_read, weight_step,
    weight_value, weight_sigmoid, filter_input, filter_write, filter_read, step_bias, rate_log,
    skip_gain, output_gain, opening_state, decay_shift, depth_filter, channel_gain,
    unproject_state, unproject_filter,
):
    n = lax.axis_size("sp")
    t = tokens.shape[1]
    hb = pl.BlockSpec(memory_space=pl.ANY)
    dma = pltpu.SemaphoreType.DMA
    steps = n // 2
    v = pltpu.VMEM
    return pl.pallas_call(
        partial(mixer_kernel, n),
        out_shape=jax.ShapeDtypeStruct((1, t // 8, CHANNELS), BF16),
        in_specs=[hb] * 22,
        out_specs=pl.BlockSpec(memory_space=pltpu.VMEM),
        scratch_shapes=[
            v((t, 2048), BF16), v((1, 2048), F32), v((4, 128), BF16),
            v((4, 256), BF16), v((4, 128), BF16), v((4, 128), BF16),
            *[pltpu.SMEM((4,), F32)] * 3,
            v((1, 256), F32), v((4, 64, 128), F32), v((4, t), F32), v((31, 256), BF16),
            v((1, 256), F32),
            v((n, t + 32, 128), BF16),
            v((n, 128, 512), BF16), v((n, 128, 256), BF16), v((n, 16, 128), BF16),
            v((n, 128, 384), BF16), v((n, 128, 128), BF16), v((n, 512, 128), BF16),
            v((t + 32, 768), F32), v((t + 32, 128), F32), v((t + 32, 512), F32),
            v((256, 256), BF16), v((31 * 8, 256), F32),
            v((32, 2048), BF16),
            v((8 + t, 512), F32), v((32 + t, 256), F32),
            v((t, 256), BF16), v((t, 128), BF16), v((t, 128), BF16), v((t, 256), BF16),
            v((128, t), F32), v((t, 128), F32), v((t, 256), F32), v((t, 256), F32),
            v((t, 128), F32),
            v((8, 8, t), F32), v((n, 128, 256), BF16), v((n, 8, 256), F32),
            v((128, 256), F32), v((128, 256), F32), v((8, 256), F32), v((t, 512), BF16),
            v((8, t, 256), F32), v((8, 4, 64, 256), BF16), v((8, 4, 64, 256), BF16),
            *[v((8, 64, 256), BF16)] * 6,
            dma((23,)), dma((3, 2, 4)), dma((7, 2, steps)),
            dma((3, 2, 4)), dma((3, 2, steps)),
            dma((2, 2)), dma((4, 2, steps)), dma((2,)), dma((2,)),
            dma((1,)), dma((1,)), dma((4,)), dma((4, 8)),
        ],
        compiler_params=pltpu.CompilerParams(
            collective_id=0, has_side_effects=True, vmem_limit_bytes=62 * 1024 * 1024),
        name="mixer",
    )(
        tokens, input_gain.reshape(1, -1), weight_input, weight_write, weight_step.T, weight_gate,
        weight_read, weight_value, weight_sigmoid, unproject_state, unproject_filter,
        filter_input, filter_write, filter_read, step_bias, rate_log, skip_gain,
        output_gain.reshape(1, -1), opening_state, decay_shift, depth_filter,
        channel_gain.reshape(1, -1),
    )


def solution(mesh):
    in_specs = (
        P("fs", "sp", None),
        P(),
        P("sp", "tp"),
        P("sp", "tp"),
        P("sp", "tp"),
        P("sp", "tp"),
        P("sp", "tp"),
        P("sp", "tp"),
        P("sp", "tp"),
        P(None, "tp"),
        P(None, "tp"),
        P(None, "tp"),
        P("tp"),
        P("tp"),
        P("tp"),
        P("tp"),
        P("fs", "tp", None, None),
        P("fs", "tp", "sp"),
        P(None, "tp"),
        P("tp"),
        P("tp", "sp"),
        P("tp", "sp"),
    )
    out_specs = P("fs", ("sp", "tp"), None)
    return jax.shard_map(
        per_device, mesh=mesh, in_specs=in_specs, out_specs=out_specs, check_vma=False
    )
```

time: 127 us -> 105 us (0.83)
  Pallas kernels: 123 us -> 103 us
  local copies, waits for them, and re-layouts: 2.95 us -> 1.67 us
    pallas_call x1, Pallas kernels: 123 us -> 103 us  [per_device(): pl.pallas_call(partial(mixer_kernel, n), out_shape=jax.ShapeDtypeStruct((...]
    pad x1 -> x0, local copies, waits for them, and re-layouts: 1.28 us -> none  [per_device(): ws = jnp.pad(weight_step.T, ((0, 16 - weight_step.shape[1]), (0, 0)))]
where the time goes in v3:
time: 105 us
  Pallas kernels  103 us (98%)
  local copies, waits for them, and re-layouts  1.67 us (2%)
    pallas_call x1, Pallas kernels, per_device(): pl.pallas_call(partial(mixer_kernel, n), out_shape=jax.ShapeDtypeStruct((...  103 us

profile of v3, /device:TPU:1, one launch (start us, length us, event | category | flops | bytes accessed | tf_op | source)
XLA Modules:
  0.0 104.6 jit_solution(7235712503228637729)
XLA Ops:
  0.0 103.0 %mixer.1 = bf16[1,64,2048]{2,1,0:T(8,128)(2,1)} custom-call(bf16[1,512,2048]{2,1,0:T(8,128)(2,1)} %tok_h.1, f32[1,2048]{1,0:T(1,128)} %bitcast.4, bf16[128,256]{1,0:T(8,128)(2,1)} %wi.1, bf16[128,128]{1,0:T(8,128)(2,1)} %ww.1, bf16[4,128]{1,0:T(4,128)(2,1)} %bitcast.5, bf16[128,256]{1,0:T(8,128)(2,1)} %wg.1, bf16[128,128]{1,0:T(8,128)(2,1)} %wr.1, ...), custom_call_target="tpu_custom_call" | custom-call | tf_op jit(solution)/shard_map/mixer/pallas_call | solution.py:608
  103.0 1.7 %copy.24 = bf16[1,64,2048]{2,1,0:T(8,128)(2,1)} copy(bf16[1,64,2048]{2,1,0:T(8,128)(2,1)} %mixer.1) | data formatting | bytes 524288

commit v4 on v3

--- a/solution.py
+++ b/solution.py
@@ -10,8 +10,8 @@
 MESH = pl.DeviceIdType.MESH
 F32, BF16 = jnp.float32, jnp.bfloat16
 CHANNELS = 2048
-OFFSETS = (0, 1, 8)
-LONG_TO_ACT = 3
+OFFSETS = (0, 2, 6)
+SHARE_LAGS = (1, 2, 2)
 
 
 def mixer_kernel(
@@ -21,11 +21,11 @@
     ch_gain_h,
     out,
     tok, gain, ws_v, f_in, f_wr, f_rd, bias, rate, skip, out_gain, opening, shift, taps, ch_gain,
-    normed, ap, aq, as_, cp, cq, up, acc_a, acc_s, acc_c, blank, tapsb,
-    tok_edge, ext4, ext31, x_ref, b_ref, c_ref, gate_ref,
+    normed, ap, aq, as_, cp, cq, up, gp, acc_a, acc_q, acc_s, acc_c, acc_g, blank, tapsb,
+    tok_edge, ext4, extq, ext31, x_ref, b_ref, c_ref,
     rows_ref, cols_ref, inside, filtered, sums_ref, stat, ebuf, tbuf, e_right, e_left, run, act,
     pbuf, d2d_src, d2d_dst, far_src, far_dst, rn_src, rn_dst, dn_src, dn_dst,
-    local_sem, zs, zr, ys, yr, es, er, hs, hr, ss, sr, os_, or_,
+    local_sem, zs, zr, ys, yr, yds, ydr, es, er, hs, hr, ss, sr, os_, or_,
 ):
     z = lax.axis_index("sp")
     y = lax.axis_index("fs")
@@ -43,9 +43,9 @@
         pl.semaphore_signal(barrier, inc=1, device_id=where, device_id_type=MESH)
 
     pairs = [
-        (ws_h, ws_v), (wi, ap.at[z, :, pl.ds(0, 256)]), (wg, ap.at[z, :, pl.ds(256, 256)]),
+        (ws_h, ws_v), (wi, ap.at[z]),
         (ww, aq.at[z, :, pl.ds(0, 128)]), (wr, aq.at[z, :, pl.ds(128, 128)]),
-        (tok_h.at[0], tok), (gain_h, gain), (wv, cp.at[z, :, pl.ds(0, 256)]),
+        (tok_h.at[0], tok), (gain_h, gain), (wg, gp.at[z]), (wv, cp.at[z, :, pl.ds(0, 256)]),
         (wsg.at[:, pl.ds(0, 128)], cp.at[z, :, pl.ds(256, 128)]),
         (wsg.at[:, pl.ds(128, 128)], cq.at[z]),
         (us, up.at[z, pl.ds(0, 256)]), (uf, up.at[z, pl.ds(256, 256)]),
@@ -66,8 +66,9 @@
         ref = blank.at[pl.ds(0, count // 512)]
         pltpu.make_async_copy(ref, ref, sem).wait()
 
-    groups = [(ap, (aq, as_)), (cp, (cq,)), (up, ())]
-    part_bytes = [ref.shape[1] // 4 * ref.shape[2] * 2 for ref, _ in groups]
+    groups = [((ap,), (aq, as_)), ((cp,), (cq,)), ((up, gp), ())]
+    q_parts = (4, 2, 0)
+    part_bytes = [sum(ref.shape[1] // 4 * ref.shape[2] * 2 for ref in two) for two, _ in groups]
     z_bytes = [p + sum(ref.shape[1] * ref.shape[2] * 2 for ref in one)
                for p, (_, one) in zip(part_bytes, groups)]
 
@@ -80,36 +81,43 @@
 
     def pieces(g, c, j):
         two, one = groups[g]
-        if c == 0:
-            return [part(two, j, y)]
-        rows = one[0].shape[1] // 2
-        more = [b.at[j] for b in one[1:]] if c == 2 else []
-        return [one[0].at[j, pl.ds((c - 1) * rows, rows)]] + more
-
-    chunks = [3 if one else 1 for _, one in groups]
+        if c < len(two):
+            return [part(two[len(two) - 1 - c], j, y)]
+        rows = one[0].shape[1] // q_parts[g]
+        more = [b.at[j] for b in one[1:]] if c == chunks[g] - 1 else []
+        return [one[0].at[j, pl.ds((c - len(two)) * rows, rows)]] + more
+
+    chunks = [len(two) + q for (two, _), q in zip(groups, q_parts)]
     first = [sum(chunks[:g]) for g in range(len(groups))]
 
     def chunk_bytes(g, c):
-        if c == 0:
-            return part_bytes[g]
-        one = groups[g][1]
-        rest = sum(r.shape[1] * r.shape[2] * 2 for r in one[1:]) if c == 2 else 0
-        return one[0].shape[1] * one[0].shape[2] + rest
+        two, one = groups[g]
+        if c < len(two):
+            ref = two[len(two) - 1 - c]
+            return ref.shape[1] // 4 * ref.shape[2] * 2
+        rest = sum(r.shape[1] * r.shape[2] * 2 for r in one[1:]) if c == chunks[g] - 1 else 0
+        return one[0].shape[1] * one[0].shape[2] * 2 // q_parts[g] + rest
 
     def start_chunk(g, c, s, way):
         for r in pieces(g, c, shard(s - 1, way)):
-            remote(r, r, zs.at[g, way, lax.rem(s, 4)], zr.at[first[g] + c, way, s - 1],
+            remote(r, r, zs.at[g, way, lax.rem(s, 4)], zr.at[first[g] + c, way, lax.rem(s, 4)],
                    {"sp": z_next if way == 0 else z_prev}).start()
 
     y_far = lax.rem(y + 2, 4)
-    direct_from = n_right - 1
+    direct_from = n_right
+    finals = (n_right + 1, n_right + 3, n_right + 3)
 
     def y_start(g, s, way, kind, q):
         up_way = kind == 0 or (kind == 2 and way == 0)
-        r = part(groups[g][0], shard(s, way), q)
         k = kind // 2
         where = y_far if kind == 3 else (y_next if up_way else y_prev)
-        remote(r, r, ys.at[g, k, lax.rem(s, 4)], yr.at[g, k, s - 1], {"fs": where}).start()
+        for ref in groups[g][0]:
+            r = part(ref, shard(s, way), q)
+            if kind == 3:
+                remote(r, r, yds.at[g], ydr.at[g], {"fs": where}).start()
+            else:
+                remote(r, r, ys.at[g, k, lax.rem(s, 4)], yr.at[g, k, s - 1],
+                       {"fs": where}).start()
 
     def y_wait(sem, g, s, per_way):
         @pl.when(s <= n_left)
@@ -127,13 +135,13 @@
 
                 @pl.when((s >= 1) & (s <= last))
                 def _():
-                    wait_bytes(zr.at[first[g] + c, way, s - 1], chunk_bytes(g, c))
+                    wait_bytes(zr.at[first[g] + c, way, lax.rem(s, 4)], chunk_bytes(g, c))
 
                 @pl.when(s < last)
                 def _():
                     start_chunk(g, c, s + 1, way)
 
-                if c == 0:
+                if c == len(groups[g][0]) - 1:
                     @pl.when((s >= 1) & (s <= last))
                     def _():
                         y_start(g, s, way, 0, y)
@@ -152,43 +160,65 @@
                 wait_bytes(zs.at[g, 1, lax.rem(s - 2, 4)], z_bytes[g])
 
     def share(g, s):
-        @pl.when((s >= 2) & (s <= n_right + 1))
-        def _():
-            y_wait(yr.at[g, 0, s - 2], g, s - 1, 2)
-
-            @pl.when(s - 1 < direct_from)
-            def _():
-                y_start(g, s - 1, 0, 2, y_prev)
-                y_start(g, s - 1, 1, 2, y_next)
+        lag = SHARE_LAGS[g]
+        final = finals[g]
+
+        @pl.when((s >= 1 + lag) & (s <= n_right + lag))
+        def _():
+            y_wait(yr.at[g, 0, s - lag - 1], g, s - lag, 2)
+            y_wait(ys.at[g, 0, lax.rem(s - lag, 4)], g, s - lag, 2)
+
+            @pl.when(s - lag < direct_from)
+            def _():
+                y_start(g, s - lag, 0, 2, y_prev)
+                y_start(g, s - lag, 1, 2, y_next)
+
+        @pl.when((s >= 2 + lag) & (s <= direct_from + lag))
+        def _():
+            wait_bytes(ys.at[g, 1, lax.rem(s - lag - 1, 4)], 2 * part_bytes[g])
 
         def complete(k, carry):
-            y_wait(yr.at[g, 1, k - 1], g, k, 1)
-            y_wait(ys.at[g, 0, lax.rem(k, 4)], g, k, 2)
-            y_wait(ys.at[g, 1, lax.rem(k, 4)], g, k, 1)
-            if g < 2:
-                with jax.named_scope("mm"):
-                    multiply(g, k)
+            @pl.when(k < direct_from)
+            def _():
+                wait_bytes(yr.at[g, 1, k - 1], 2 * part_bytes[g])
+
+            @pl.when(k == direct_from)
+            def _():
+                wait_bytes(ydr.at[g], part_bytes[g])
+                wait_bytes(yds.at[g], part_bytes[g])
+
+            with jax.named_scope("mm"):
+                multiply(g, k)
             return carry
 
-        @pl.when((s >= 4) & (s <= n_right + 2))
-        def _():
-            low = jnp.where(s > n_right + 1, s - 2, s - 3)
-            high = jnp.where(s > n_right, s - 2, s - 3)
+        @pl.when((s >= 3 + lag) & (s <= final))
+        def _():
+            low, high = s - 2 - lag, jnp.where(s == final, n_right, s - 2 - lag)
+            if g == 0:
+                low = jnp.where(s == final, low + 1, low)
+                high = jnp.where(s == final - 1, high + 1, high)
             lax.fori_loop(low, high + 1, complete, 0)
 
     def both(ref, j1, j2, axis):
         return jnp.concatenate([ref[j1], ref[j2]], axis=axis)
 
-    def multiply(g, k):
+    def rows_at(k):
         j1 = jnp.where(k == n_right, z, shard(k, 0))
         j2 = shard(k, 1)
-        rows = both(normed, j1, j2, 1)
+        return j1, j2, both(normed, j1, j2, 1)
+
+    def multiply_early(k):
+        j1, j2, rows = rows_at(k)
+        acc_q[...] += jnp.dot(rows, both(aq, j1, j2, 0), preferred_element_type=F32)
+        acc_s[:, :16] += lax.dot_general(
+            rows, both(as_, j1, j2, 1), (((1,), (1,)), ((), ())), preferred_element_type=F32)
+
+    def multiply(g, k):
+        j1, j2, rows = rows_at(k)
         if g == 0:
-            w = jnp.concatenate([both(ap, j1, j2, 0), both(aq, j1, j2, 0)], axis=1)
-            acc_a[...] += jnp.dot(rows, w, preferred_element_type=F32)
-            acc_s[:, :16] += lax.dot_general(
-                rows, both(as_, j1, j2, 1), (((1,), (1,)), ((), ())),
-                preferred_element_type=F32)
+            acc_a[...] += jnp.dot(rows, both(ap, j1, j2, 0), preferred_element_type=F32)
+        elif g == 2:
+            acc_g[...] += jnp.dot(rows[:t_rows], both(gp, j1, j2, 0), preferred_element_type=F32)
         else:
             w = jnp.concatenate([both(cp, j1, j2, 0), both(cq, j1, j2, 0)], axis=1)
             acc_c[...] += jnp.dot(rows, w, preferred_element_type=F32)
@@ -203,11 +233,11 @@
         ref = tok_edge.at[:, edge_lanes]
         return remote(ref, ref, hs.at[1], hr.at[1], {"tp": lax.rem(tp + i, 8)})
 
-    def short_filter(lo, hi, kernel, target):
+    def short_filter(source, lo, hi, kernel, target):
         weights = [kernel[k:k + 1, :].astype(F32) for k in range(4)]
 
         def strip(i, carry):
-            block = ext4[pl.ds(pl.multiple_of(i * 64, 64), 72), lo:hi]
+            block = source[pl.ds(pl.multiple_of(i * 64, 64), 72), lo:hi]
             total = weights[0] * pltpu.roll(block, 72 - 5, 0)[:64]
             for k in range(1, 4):
                 total = total + weights[k] * pltpu.roll(block, 72 - 5 - k, 0)[:64]
@@ -217,15 +247,9 @@
 
         lax.fori_loop(0, t_rows // 64, strip, 0)
 
-    def finish_a():
-        mapped = acc_a[...].astype(BF16)
-        own_rows = mapped[:t_rows]
-        edge = jnp.where(z > 0, acc_a[t_rows + 24:, :].astype(BF16).astype(F32), 0.0)
-        ext4[0:8, 0:256] = edge[:, 0:256]
-        ext4[0:8, 256:512] = edge[:, 512:768]
-        ext4[8:, 0:256] = own_rows[:, 0:256].astype(F32)
-        ext4[8:, 256:512] = own_rows[:, 512:768].astype(F32)
-        gate_ref[...] = own_rows[:, 256:512]
+    def extend(target, acc, lo, hi):
+        target[0:8, :] = jnp.where(z > 0, acc[t_rows + 24:, lo:hi].astype(BF16).astype(F32), 0.0)
+        target[8:, :] = acc[0:t_rows, lo:hi].astype(BF16).astype(F32)
 
     def finish_c():
         value = acc_c[:, :256].astype(BF16).astype(F32)
@@ -242,9 +266,10 @@
             [jnp.where(lane < 64, c[:, 2 * k:2 * k + 1], c[:, 2 * k + 1:2 * k + 2])
              for k in range(2)], axis=1)
 
-    def local_state():
-        short_filter(0, 256, f_in, x_ref)
-        short_filter(256, 384, f_wr, b_ref)
+    def local_rates():
+        extend(extq, acc_q, 0, 256)
+        short_filter(extq, 0, 128, f_wr, b_ref)
+        short_filter(extq, 128, 256, f_rd, c_ref)
         head = lax.broadcasted_iota(jnp.int32, (8, t_rows), 0)
         place = lax.broadcasted_iota(jnp.int32, (8, t_rows), 1)
         bias8 = jnp.zeros((8, t_rows), F32)
@@ -268,22 +293,26 @@
         rows_ref[24:32, :] = jnp.exp(total)
         rows_ref[32:, :] = jnp.zeros((96, t_rows), F32)
         cols_ref[...] = rows_ref[...].T
+        spread = jnp.concatenate(
+            [jnp.where(lane < 64, end[2 * k:2 * k + 1, :], end[2 * k + 1:2 * k + 2, :])
+             for k in range(2)], axis=1)
+        tbuf[z] = jnp.broadcast_to(spread, (8, 256))
+
+    def local_state():
+        extend(ext4, acc_a, 0, 256)
+        short_filter(ext4, 0, 256, f_in, x_ref)
         scaled = (x_ref[...].astype(F32) * by_head(16)).astype(BF16)
         ebuf[z] = lax.dot_general(
             b_ref[...], scaled, (((0,), (0,)), ((), ())), preferred_element_type=F32
         ).astype(BF16)
-        spread = jnp.concatenate(
-            [jnp.where(lane < 64, end[2 * k:2 * k + 1, :], end[2 * k + 1:2 * k + 2, :])
-             for k in range(2)], axis=1)
-        tbuf[z] = jnp.broadcast_to(spread, (8, 256))
-
-    e_bytes = (2 * 32 * 256,) * 3 + (2 * 32 * 256 + 4 * 8 * 256,)
+
+    e_bytes = (2 * 32 * 256 + 4 * 8 * 256,) + (2 * 32 * 256,) * 3
 
     def state_start(c, s, way):
         j = shard(s - 1, way)
         where = {"sp": z_next if way == 0 else z_prev}
-        for r in [ebuf.at[j, pl.ds(32 * c, 32)]] + [tbuf.at[j]] * (c // 3):
-            remote(r, r, es.at[way, lax.rem(s, 2)], er.at[c, way, s - 1], where).start()
+        for r in [ebuf.at[j, pl.ds(32 * c, 32)]] + [tbuf.at[j]] * (c == 0):
+            remote(r, r, es.at[way, lax.rem(s, 2)], er.at[c, way, lax.rem(s, 4)], where).start()
 
     def state_ring(s):
         for c in range(4):
@@ -292,7 +321,7 @@
 
                 @pl.when(s <= last)
                 def _():
-                    wait_bytes(er.at[c, way, s - 1], e_bytes[c])
+                    wait_bytes(er.at[c, way, lax.rem(s, 4)], e_bytes[c])
 
                 @pl.when(s < last)
                 def _():
@@ -388,14 +417,14 @@
 
     own[0].wait()
     as_[z] = jnp.concatenate([ws_v[...].astype(F32), jnp.zeros((12, 128), F32)]).astype(BF16)
-    for c in own[1:5]:
+    for c in own[1:4]:
         c.wait()
     with jax.named_scope("entry"):
         pl.semaphore_wait(barrier, len(greet))
     for c in range(chunks[0]):
         start_chunk(0, c, 1, 0)
         start_chunk(0, c, 1, 1)
-    for c in own[5:]:
+    for c in own[4:]:
         c.wait()
 
     border().start()
@@ -417,26 +446,35 @@
     e_right[...] = jnp.zeros_like(e_right)
     run[...] = jnp.zeros_like(run)
     e_left[...] = opening[...].reshape(256, 128).T
-    for acc in (acc_a, acc_s, acc_c):
+    for acc in (acc_a, acc_q, acc_s, acc_c, acc_g):
         acc[...] = jnp.zeros_like(acc)
     for k in range(taps.shape[0]):
         tapsb[8 * k:8 * k + 8, :] = jnp.broadcast_to(
             taps[k:k + 1, :].astype(F32), (8, 256))
 
-    done = [n_right + 2 + o for o in OFFSETS]
+    done = [f + o for f, o in zip(finals, OFFSETS)]
     state_at = done[0]
     long_at = done[1] + 1
-    acts_at = long_at + LONG_TO_ACT
-    last_slot = max(max(done), state_at + n_right, state_at + 5, acts_at) + 1
+    last_slot = max(max(done), state_at + n_right, state_at + 5, long_at + 2) + 1
+
+    assert long_at + 1 < state_at + n_right and last_slot == state_at + n_right + 1
+
+    def at_step(g, t):
+        return t - OFFSETS[g] - (jnp.where(t > state_at, 0, 1) if g == 2 else 0)
 
     def slot(t, carry):
+        @pl.when(t == state_at + n_right)
+        def _():
+            with jax.named_scope("fact"):
+                filter_act()
+
         @pl.when((t > state_at) & (t <= state_at + n_right))
         def _():
             with jax.named_scope("ring"):
                 state_ring(t - state_at)
 
         for g in range(3):
-            s = t - OFFSETS[g]
+            s = at_step(g, t)
             low = 1 if g == 0 else 0
 
             @pl.when((s >= low) & (s <= n_right + 2))
@@ -455,10 +493,38 @@
             wait_bytes(hr.at[1], 7 * 32 * 256 * 2)
             norm_rows(tok_edge, pl.ds(0, 32), pl.ds(t_rows, 32))
 
+        def early(k, carry):
+            multiply_early(k)
+            return carry
+
+        @pl.when((t >= 3) & (t <= n_right))
+        def _():
+            with jax.named_scope("mmq"):
+                lax.fori_loop(jnp.where(t == 3, 1, t), t + 1, early, 0)
+
+        @pl.when(t == n_right + 1)
+        def _():
+            with jax.named_scope("rates"):
+                local_rates()
+
+        for i in range(4):
+            @pl.when(t == state_at + 1 + i)
+            def _():
+                with jax.named_scope("inside"):
+                    inside_strip(i)
+
+        for i in range(2):
+            @pl.when(t == long_at + i)
+            def _():
+                with jax.named_scope("longf"):
+                    long_filter(i)
+                    if i == 1:
+                        send_sums()
+
         for g in range(3):
-            s = t - OFFSETS[g]
-
-            @pl.when((s >= 2) & (s <= n_right + 2))
+            s = at_step(g, t)
+
+            @pl.when((s >= 2) & (s <= finals[g]))
             def _():
                 with jax.named_scope("share%d" % g):
                     share(g, s)
@@ -466,43 +532,18 @@
         @pl.when(t == state_at)
         def _():
             with jax.named_scope("lstate"):
-                finish_a()
                 local_state()
             for c in range(4):
                 for way in (0, 1):
                     state_start(c, 1, way)
+            with jax.named_scope("extra"):
+                comm(2, state_at - OFFSETS[2])
+                share(2, state_at - OFFSETS[2])
 
         @pl.when(t == done[1])
         def _():
             with jax.named_scope("fin_c"):
                 finish_c()
-
-        @pl.when(t == state_at + 1)
-        def _():
-            with jax.named_scope("read"):
-                short_filter(384, 512, f_rd, c_ref)
-
-        for i in range(4):
-            @pl.when(t == state_at + 2 + i)
-            def _():
-                with jax.named_scope("inside"):
-                    inside_strip(i)
-
-        @pl.when(t == long_at)
-        def _():
-            with jax.named_scope("longf"):
-                long_filter(0)
-
-        @pl.when(t == long_at + 1)
-        def _():
-            with jax.named_scope("longf"):
-                long_filter(1)
-                send_sums()
-
-        @pl.when(t == acts_at)
-        def _():
-            with jax.named_scope("fact"):
-                filter_act()
         return carry
 
     lax.fori_loop(1, last_slot, slot, 0)
@@ -514,7 +555,7 @@
         at = slice(128 * i, 128 * i + 128)
         carried = jnp.dot(c_ref[at, :], entering, preferred_element_type=F32)
         v = inside[at, :] + by_head(24, at) * carried
-        g = gate_ref[at, :].astype(F32)
+        g = acc_g[at, :].astype(BF16).astype(F32)
         v = v * (g * jax.nn.sigmoid(g))
         v = v * lax.rsqrt(jnp.mean(v * v, axis=-1, keepdims=True) + 1e-06)
         act[at, 0:256] = (v * out_gain[...]).astype(BF16)
@@ -580,14 +621,14 @@
             with jax.named_scope("o_mm"):
                 stage_multiply(i)
 
-        for lag, stage in ((2, stage_pair), (5, stage_relay), (6, stage_direct), (9, stage_out)):
+        for lag, stage in ((3, stage_pair), (9, stage_direct), (10, stage_relay), (18, stage_out)):
             @pl.when((i >= lag) & (i < blocks + lag))
             def _():
                 with jax.named_scope("o_st%d" % lag):
                     stage(i - lag)
         return carry
 
-    lax.fori_loop(0, blocks + 9, out_slot, 0)
+    lax.fori_loop(0, blocks + 18, out_slot, 0)
     with jax.named_scope("o_end"):
         for k, r in enumerate((d2d_src, far_src, rn_src, dn_src)):
             pltpu.make_async_copy(r, r, os_.at[k]).wait()
@@ -617,22 +658,24 @@
             v((1, 256), F32), v((4, 64, 128), F32), v((4, t), F32), v((31, 256), BF16),
             v((1, 256), F32),
             v((n, t + 32, 128), BF16),
-            v((n, 128, 512), BF16), v((n, 128, 256), BF16), v((n, 16, 128), BF16),
+            v((n, 128, 256), BF16), v((n, 128, 256), BF16), v((n, 16, 128), BF16),
             v((n, 128, 384), BF16), v((n, 128, 128), BF16), v((n, 512, 128), BF16),
-            v((t + 32, 768), F32), v((t + 32, 128), F32), v((t + 32, 512), F32),
-            v((256, 256), BF16), v((31 * 8, 256), F32),
+            v((n, 128, 256), BF16),
+            v((t + 32, 256), F32), v((t + 32, 256), F32), v((t + 32, 128), F32), v((t + 32, 512), F32),
+            v((t, 256), F32),
+            v((384, 256), BF16), v((31 * 8, 256), F32),
             v((32, 2048), BF16),
-            v((8 + t, 512), F32), v((32 + t, 256), F32),
-            v((t, 256), BF16), v((t, 128), BF16), v((t, 128), BF16), v((t, 256), BF16),
+            v((8 + t, 256), F32), v((8 + t, 256), F32), v((32 + t, 256), F32),
+            v((t, 256), BF16), v((t, 128), BF16), v((t, 128), BF16),
             v((128, t), F32), v((t, 128), F32), v((t, 256), F32), v((t, 256), F32),
             v((t, 128), F32),
             v((8, 8, t), F32), v((n, 128, 256), BF16), v((n, 8, 256), F32),
             v((128, 256), F32), v((128, 256), F32), v((8, 256), F32), v((t, 512), BF16),
             v((8, t, 256), F32), v((8, 4, 64, 256), BF16), v((8, 4, 64, 256), BF16),
             *[v((8, 64, 256), BF16)] * 6,
-            dma((23,)), dma((3, 2, 4)), dma((7, 2, steps)),
-            dma((3, 2, 4)), dma((3, 2, steps)),
-            dma((2, 2)), dma((4, 2, steps)), dma((2,)), dma((2,)),
+            dma((23,)), dma((3, 2, 4)), dma((10, 2, 4)),
+            dma((3, 2, 4)), dma((3, 2, steps)), dma((3,)), dma((3,)),
+            dma((2, 2)), dma((4, 2, 4)), dma((2,)), dma((2,)),
             dma((1,)), dma((1,)), dma((4,)), dma((4, 8)),
         ],
         compiler_params=pltpu.CompilerParams(

time: 105 us -> 98.4 us (0.937)
  Pallas kernels: 103 us -> 96.6 us
    pallas_call x1, Pallas kernels: 103 us -> 96.6 us  [per_device(): pl.pallas_call(partial(mixer_kernel, n), out_shape=jax.ShapeDtypeStruct((...]
where the time goes in v4:
time: 98.4 us; the launch traced here: 98.3 us
  Pallas kernels  96.6 us (98%)
  local copies, waits for them, and re-layouts  1.67 us (2%)
    pallas_call x1, Pallas kernels, per_device(): pl.pallas_call(partial(mixer_kernel, n), out_shape=jax.ShapeDtypeStruct((...  96.6 us

profile of v4, /device:TPU:1, one launch (start us, length us, event | category | flops | bytes accessed | tf_op | source)
XLA Modules:
  0.0 98.3 jit_solution(16968521037742846200)
XLA Ops:
  0.0 96.6 %mixer.1 = bf16[1,64,2048]{2,1,0:T(8,128)(2,1)} custom-call(bf16[1,512,2048]{2,1,0:T(8,128)(2,1)} %tok_h.1, f32[1,2048]{1,0:T(1,128)} %bitcast.4, bf16[128,256]{1,0:T(8,128)(2,1)} %wi.1, bf16[128,128]{1,0:T(8,128)(2,1)} %ww.1, bf16[4,128]{1,0:T(4,128)(2,1)} %bitcast.5, bf16[128,256]{1,0:T(8,128)(2,1)} %wg.1, bf16[128,128]{1,0:T(8,128)(2,1)} %wr.1, ...), custom_call_target="tpu_custom_call" | custom-call | tf_op jit(solution)/shard_map/mixer/pallas_call | solution.py:649
  96.6 1.7 %copy.24 = bf16[1,64,2048]{2,1,0:T(8,128)(2,1)} copy(bf16[1,64,2048]{2,1,0:T(8,128)(2,1)} %mixer.1) | data formatting | bytes 524288

commit v5 on v4

--- a/solution.py
+++ b/solution.py
@@ -21,7 +21,7 @@
     ch_gain_h,
     out,
     tok, gain, ws_v, f_in, f_wr, f_rd, bias, rate, skip, out_gain, opening, shift, taps, ch_gain,
-    normed, ap, aq, as_, cp, cq, up, gp, acc_a, acc_q, acc_s, acc_c, acc_g, blank, tapsb,
+    normed, ap, aq, as_, cp, cq, up, uq, gp, acc_a, acc_q, acc_s, acc_c, acc_g, blank, tapsb,
     tok_edge, ext4, extq, ext31, x_ref, b_ref, c_ref,
     rows_ref, cols_ref, inside, filtered, sums_ref, stat, ebuf, tbuf, e_right, e_left, run, act,
     pbuf, d2d_src, d2d_dst, far_src, far_dst, rn_src, rn_dst, dn_src, dn_dst,
@@ -48,7 +48,8 @@
         (tok_h.at[0], tok), (gain_h, gain), (wg, gp.at[z]), (wv, cp.at[z, :, pl.ds(0, 256)]),
         (wsg.at[:, pl.ds(0, 128)], cp.at[z, :, pl.ds(256, 128)]),
         (wsg.at[:, pl.ds(128, 128)], cq.at[z]),
-        (us, up.at[z, pl.ds(0, 256)]), (uf, up.at[z, pl.ds(256, 256)]),
+        (us, up.at[z, pl.ds(0, 256)]), (uf.at[pl.ds(0, 192)], up.at[z, pl.ds(256, 192)]),
+        (uf.at[pl.ds(192, 64)], uq.at[z]),
         (f_in_h, f_in), (f_wr_h, f_wr), (f_rd_h, f_rd), (bias_h, bias), (rate_h, rate),
         (skip_h, skip), (out_gain_h, out_gain), (opening_h.at[0], opening),
         (shift_h.at[0], shift), (taps_h, taps), (ch_gain_h, ch_gain),
@@ -66,8 +67,8 @@
         ref = blank.at[pl.ds(0, count // 512)]
         pltpu.make_async_copy(ref, ref, sem).wait()
 
-    groups = [((ap,), (aq, as_)), ((cp,), (cq,)), ((up, gp), ())]
-    q_parts = (4, 2, 0)
+    groups = [((ap,), (aq, as_)), ((cp,), (cq,)), ((up, gp), (uq,))]
+    q_parts = (4, 2, 1)
     part_bytes = [sum(ref.shape[1] // 4 * ref.shape[2] * 2 for ref in two) for two, _ in groups]
     z_bytes = [p + sum(ref.shape[1] * ref.shape[2] * 2 for ref in one)
                for p, (_, one) in zip(part_bytes, groups)]
@@ -585,7 +586,8 @@
                       at_x(3 + 2 * lax.rem(b, 2)))
 
     def stage_multiply(b):
-        w = both(up, 2 * b, 2 * b + 1, 1)
+        w = jnp.concatenate(
+            [both(up, 2 * b, 2 * b + 1, 1), both(uq, 2 * b, 2 * b + 1, 1)], axis=0)
         pbuf[b] = jnp.dot(act[...], w, preferred_element_type=F32)
         for xx in range(4):
             d2d_src[b, xx] = pbuf[b, rows_of(xx, 1 - core), :].astype(BF16)
@@ -659,11 +661,11 @@
             v((1, 256), F32),
             v((n, t + 32, 128), BF16),
             v((n, 128, 256), BF16), v((n, 128, 256), BF16), v((n, 16, 128), BF16),
-            v((n, 128, 384), BF16), v((n, 128, 128), BF16), v((n, 512, 128), BF16),
+            v((n, 128, 384), BF16), v((n, 128, 128), BF16), v((n, 448, 128), BF16), v((n, 64, 128), BF16),
             v((n, 128, 256), BF16),
             v((t + 32, 256), F32), v((t + 32, 256), F32), v((t + 32, 128), F32), v((t + 32, 512), F32),
             v((t, 256), F32),
-            v((384, 256), BF16), v((31 * 8, 256), F32),
+            v((384, 128), F32), v((31 * 8, 256), F32),
             v((32, 2048), BF16),
             v((8 + t, 256), F32), v((8 + t, 256), F32), v((32 + t, 256), F32),
             v((t, 256), BF16), v((t, 128), BF16), v((t, 128), BF16),
@@ -673,7 +675,7 @@
             v((128, 256), F32), v((128, 256), F32), v((8, 256), F32), v((t, 512), BF16),
             v((8, t, 256), F32), v((8, 4, 64, 256), BF16), v((8, 4, 64, 256), BF16),
             *[v((8, 64, 256), BF16)] * 6,
-            dma((23,)), dma((3, 2, 4)), dma((10, 2, 4)),
+            dma((24,)), dma((3, 2, 4)), dma((11, 2, 4)),
             dma((3, 2, 4)), dma((3, 2, steps)), dma((3,)), dma((3,)),
             dma((2, 2)), dma((4, 2, 4)), dma((2,)), dma((2,)),
             dma((1,)), dma((1,)), dma((4,)), dma((4, 8)),

time: 98.4 us -> 98.5 us (level)
  no operation moved by 1% of the time
where the time goes in v5:
time: 98.5 us; the launch traced here: 98.3 us
  Pallas kernels  96.6 us (98%)
  local copies, waits for them, and re-layouts  1.67 us (2%)
    pallas_call x1, Pallas kernels, per_device(): pl.pallas_call(partial(mixer_kernel, n), out_shape=jax.ShapeDtypeStruct((...  96.6 us

profile of v5, /device:TPU:1, one launch (start us, length us, event | category | flops | bytes accessed | tf_op | source)
XLA Modules:
  0.0 98.3 jit_solution(918536497105110132)
XLA Ops:
  0.0 96.6 %mixer.1 = bf16[1,64,2048]{2,1,0:T(8,128)(2,1)} custom-call(bf16[1,512,2048]{2,1,0:T(8,128)(2,1)} %tok_h.1, f32[1,2048]{1,0:T(1,128)} %bitcast.4, bf16[128,256]{1,0:T(8,128)(2,1)} %wi.1, bf16[128,128]{1,0:T(8,128)(2,1)} %ww.1, bf16[4,128]{1,0:T(4,128)(2,1)} %bitcast.5, bf16[128,256]{1,0:T(8,128)(2,1)} %wg.1, bf16[128,128]{1,0:T(8,128)(2,1)} %wr.1, ...), custom_call_target="tpu_custom_call" | custom-call | tf_op jit(solution)/shard_map/mixer/pallas_call | solution.py:651
  96.6 1.7 %copy.24 = bf16[1,64,2048]{2,1,0:T(8,128)(2,1)} copy(bf16[1,64,2048]{2,1,0:T(8,128)(2,1)} %mixer.1) | data formatting | bytes 524288
